TPU v7x, 32 devices: a whole 2x2x4 slice. The times are simulated.
32 devices in a mesh: sp: 4 (over z), fs: 4 (over y, x), tp: 2 (over core).
Axes of the slice: x: 2, y: 2, z: 4, core: 2. Of those that a mesh axis runs over, the one named last changes fastest.
Arguments:
- tokens: bfloat16 [4, 512, 4096], P('fs', 'sp'), may hold values from -6 to 6
- norm_gain: float32 [4096], replicated, may hold values from 0.1 to 1.9
- pool_proj: bfloat16 [4096, 1024], P(('sp', 'fs'), 'tp'), may hold values from -0.09375 to 0.09375
- query_proj: bfloat16 [4096, 1024], P(('sp', 'fs'), 'tp'), may hold values from -0.09375 to 0.09375
- key_proj: bfloat16 [4096, 1024], P(('sp', 'fs'), 'tp'), may hold values from -0.09375 to 0.09375
- value_proj: bfloat16 [4096, 1024], P(('sp', 'fs'), 'tp'), may hold values from -0.09375 to 0.09375
- pool_map: bfloat16 [4, 256, 256], replicated, may hold values from -0.375 to 0.375
- pool_scale: float32 [1024], replicated, may hold values from 0.1 to 1.9
- decay_rate: float32 [4], P('tp'), may hold values from 2e-05 to 0.034
- start_state: float32 [4, 4, 256, 256], P('fs', 'tp', 'sp'), may hold values from -96 to 96
- pool_back: bfloat16 [1024, 4096], P('tp', ('sp', 'fs')), may hold values from -0.125 to 0.125
- retention_back: bfloat16 [1024, 4096], P('tp', ('sp', 'fs')), may hold values from -0.125 to 0.125
Outputs:
- mixed: bfloat16 [4, 512, 4096], P('fs', ('sp', 'tp'))
All inputs are finite; a program needn't handle non-finite values.
Results may differ from a plain program's by a relative error of at most 0.014.
Values may be sent and summed in bfloat16 or wider, within the bound.
A program may use at most 128 MiB of HBM per device.

v0:
```python
import jax
import jax.numpy as jnp
from jax import lax
from jax.sharding import PartitionSpec as P

GROUPS = 4
BLOCK = 128
HALO = 16


eps = 1e-06
rope_base = 10000.0
highest_precision = lax.Precision.HIGHEST
window_list = (2, 4, 8, 16)


def shortened(x):
    return jax.tree.map(lambda a: a.astype(jnp.bfloat16) if a.dtype == jnp.float32 else a, x)


def shifted(x, axis, by):
    devices = lax.axis_size(axis)
    pairs = [(i, i + by) for i in range(devices) if 0 <= i + by < devices]
    return lax.ppermute(x, axis, pairs)


def carried_in(value, axis, join, neutral):
    count, mine = (lax.axis_size(axis), lax.axis_index(axis))
    pieces = jax.tree.map(lambda part: lax.all_gather(part, axis), value)
    running = jax.tree.map(
        lambda part, zero: jnp.full_like(part, 0) + jnp.asarray(zero, part.dtype), value, neutral
    )

    def turn(position, running):
        longer = join(running, jax.tree.map(lambda part: part[position], pieces))
        return jax.tree.map(lambda new, old: jnp.where(position < mine, new, old), longer, running)

    return lax.fori_loop(0, count - 1, turn, running)


def rotate(values, positions):
    half_dim = values.shape[-1] // 2
    inv_freq = 1.0 / rope_base ** jnp.linspace(0.0, 1.0, half_dim, dtype=jnp.float32)
    angles = positions.astype(jnp.float32)[:, None] * inv_freq[None, :]
    cosine = jnp.cos(angles)[:, None, :]
    sine = jnp.sin(angles)[:, None, :]
    first_half = values[..., :half_dim]
    second_half = values[..., half_dim:]
    return jnp.concatenate(
        [first_half * cosine - second_half * sine, first_half * sine + second_half * cosine],
        axis=-1,
    )


def trailing_sums(extended, length):
    begin = extended.shape[0] - length
    running = extended[begin:]
    results = []
    for behind in range(1, 16):
        running = running + extended[begin - behind : begin - behind + length]
        if behind + 1 in window_list:
            results.append(running)
    return results


def reshape_blocks(array):
    return array.reshape((array.shape[0] // BLOCK, BLOCK) + array.shape[1:])


def block_retention(queries, keys_in, values_in, decay_rate, initial):
    length, head_count, head_dim = queries.shape
    within = jnp.arange(BLOCK, dtype=jnp.float32)
    distance = within[:, None] - within[None, :]
    decay_mask = jnp.where(
        distance[None] >= 0,
        jnp.exp(-jnp.maximum(distance, 0.0)[None] * decay_rate[:, None, None]),
        0.0,
    )
    query_decay_factor = jnp.exp(-(within + 1.0)[:, None] * decay_rate[None, :])
    key_decay_factor = jnp.exp(-(BLOCK - 1.0 - within)[:, None] * decay_rate[None, :])
    block_decay_factor = jnp.exp(-BLOCK * decay_rate)

    def advance(state_carry, inputs):
        block_queries, block_keys, block_values = inputs
        scores = (
            jnp.einsum("ihk,jhk->hij", block_queries, block_keys, precision=highest_precision)
            * decay_mask
        )
        inside = jnp.einsum("hij,jhv->ihv", scores, block_values, precision=highest_precision)
        across_blocks = jnp.einsum(
            "bzy,zyx->bzx",
            block_queries * query_decay_factor[:, :, None],
            state_carry,
            precision=highest_precision,
        )
        state_carry = state_carry * block_decay_factor[:, None, None] + jnp.einsum(
            "flm,fld->lmd",
            block_keys * key_decay_factor[:, :, None],
            block_values,
            precision=highest_precision,
        )
        return (state_carry, inside + across_blocks)

    final_state, outputs = lax.scan(
        advance,
        initial,
        (reshape_blocks(queries), reshape_blocks(keys_in), reshape_blocks(values_in)),
    )
    return (outputs.reshape(length, head_count, values_in.shape[-1]), final_state)


def combine_states(earlier, latter):
    return (earlier[0] * latter[0], latter[0][:, None, None] * earlier[1] + latter[1])


def on_device(
    tokens,
    norm_gain,
    pool_proj,
    query_proj,
    key_proj,
    value_proj,
    pool_map,
    pool_scale,
    decay_rate,
    start_state,
    pool_back,
    retention_back,
):
    sequence = tokens[0]
    length = sequence.shape[0]
    tp_index = lax.axis_index("tp")
    sp_index = lax.axis_index("sp")
    tp_count = lax.axis_size("tp")
    floats = sequence.astype(jnp.float32)
    normed = (
        floats * lax.rsqrt(jnp.mean(floats * floats, axis=-1, keepdims=True) + eps) * norm_gain
    ).astype(jnp.bfloat16)
    group_normed = lax.all_gather(normed, "fs", axis=0, tiled=True)
    quarters = (
        lax.all_to_all(pool_proj, "fs", split_axis=1, concat_axis=0, tiled=True),
        lax.all_to_all(query_proj, "fs", split_axis=1, concat_axis=0, tiled=True),
        lax.all_to_all(key_proj, "fs", split_axis=1, concat_axis=0, tiled=True),
        lax.all_to_all(value_proj, "fs", split_axis=1, concat_axis=0, tiled=True),
    )
    pieces = (
        lax.all_gather(quarters[0], "sp", axis=0, tiled=True),
        lax.all_gather(quarters[1], "sp", axis=0, tiled=True),
        lax.all_gather(quarters[2], "sp", axis=0, tiled=True),
        lax.all_gather(quarters[3], "sp", axis=0, tiled=True),
    )
    partial_cols = tuple(
        (jnp.dot(group_normed, piece_w, preferred_element_type=jnp.float32) for piece_w in pieces)
    )
    rounded = tuple((result.astype(jnp.bfloat16) for result in partial_cols))
    pool_in, query_bf, key_bf, value_bf = jax.tree.map(
        lambda part, own: part.astype(own.dtype),
        lax.all_to_all(shortened(rounded), "fs", split_axis=0, concat_axis=1, tiled=True),
        rounded,
    )
    positions = jnp.arange(length, dtype=jnp.int32) + sp_index * length
    before = shifted(pool_in[length - HALO :], "sp", 1)
    extended = jnp.concatenate([before, pool_in], axis=0).astype(jnp.float32)
    stacked = jnp.stack(trailing_sums(extended, length))
    local_groups = GROUPS // tp_count
    channels = pool_in.shape[1]
    group_dim = channels // local_groups
    group_maps = lax.dynamic_slice_in_dim(pool_map, tp_index * local_groups, local_groups, 0)
    scales = lax.dynamic_slice_in_dim(pool_scale, tp_index * channels, channels, 0)
    windows = jnp.array(window_list, dtype=jnp.int32)
    pieces = []
    for group_idx in range(local_groups):
        chosen_group = tp_index * local_groups + group_idx
        lower = group_idx * group_dim
        chosen = lax.dynamic_index_in_dim(stacked, chosen_group, 0, keepdims=False)[
            :, lower : lower + group_dim
        ]
        counts = jnp.minimum(windows[chosen_group], positions + 1).astype(jnp.float32)
        inputs = extended[HALO:, lower : lower + group_dim]
        differ = (chosen / counts[:, None] - inputs).astype(jnp.bfloat16)
        pieces.append(jnp.dot(differ, group_maps[group_idx], preferred_element_type=jnp.float32))
    pool_out = (jnp.concatenate(pieces, axis=1) * scales).astype(jnp.bfloat16)
    head_count = decay_rate.shape[0]
    head_dim = query_bf.shape[1] // head_count
    queries = rotate(query_bf.astype(jnp.float32).reshape(length, head_count, head_dim), positions)
    keys_in = rotate(
        key_bf.astype(jnp.float32).reshape(length, head_count, head_dim), positions
    ) * head_dim ** (-0.5)
    values_in = value_bf.astype(jnp.float32).reshape(length, head_count, head_dim)
    zeros_state = jnp.zeros((head_count, head_dim, head_dim), jnp.float32)
    local_output, local_state = block_retention(
        queries, keys_in, values_in, decay_rate, zeros_state
    )
    span_decay = jnp.exp(-decay_rate * length)
    whole_start = lax.all_gather(start_state, "sp", axis=2, tiled=True)[0]
    span_factor, carried_over = carried_in(
        (span_decay, local_state), "sp", combine_states, (jnp.ones_like(span_decay), zeros_state)
    )
    offset_float = (sp_index * length).astype(jnp.float32)
    carried_over = carried_over + jnp.exp(-decay_rate * offset_float)[:, None, None] * whole_start
    steps_in = jnp.arange(length, dtype=jnp.float32) + 1.0
    query_rows_scaled = queries * jnp.exp(-steps_in[:, None] * decay_rate[None, :])[:, :, None]
    retained_output = local_output + jnp.einsum(
        "lpi,pib->lpb", query_rows_scaled, carried_over, precision=highest_precision
    )
    retained_output = retained_output * lax.rsqrt(
        jnp.mean(retained_output * retained_output, axis=-1, keepdims=True) + eps
    )
    ret_out = retained_output.reshape(length, head_count * head_dim).astype(jnp.bfloat16)
    pool_cols, retention_cols = (
        lax.all_gather(pool_back, ("sp", "fs"), axis=1, tiled=True),
        lax.all_gather(retention_back, ("sp", "fs"), axis=1, tiled=True),
    )
    weight_local = jnp.concatenate([pool_cols, retention_cols], axis=0)
    joined = jnp.concatenate([pool_out, ret_out], axis=1)
    mixed = lax.psum_scatter(
        jnp.dot(joined, weight_local, preferred_element_type=jnp.float32).astype(jnp.bfloat16),
        "tp",
        scatter_dimension=0,
        tiled=True,
    )
    return mixed[None]


def solution(mesh):
    placed = (
        P("fs", "sp", None),
        P(),
        P(("sp", "fs"), "tp"),
        P(("sp", "fs"), "tp"),
        P(("sp", "fs"), "tp"),
        P(("sp", "fs"), "tp"),
        P(),
        P(),
        P("tp"),
        P("fs", "tp", "sp", None),
        P("tp", ("sp", "fs")),
        P("tp", ("sp", "fs")),
    )
    return jax.shard_map(
        on_device,
        mesh=mesh,
        in_specs=placed,
        out_specs=P("fs", ("sp", "tp"), None),
        check_vma=False,
    )
```

profile of v0, /device:TPU:30, one launch (start us, length us, event | category | flops | bytes accessed | tf_op | source)
XLA Modules:
  0.0 430.5 jit_solution(100196734017617633)
XLA Ops:
  6.5 1.2 copy.58
  7.7 7.7 %all_to_all.137 = bf16[256,4,128]{0,2,1:T(8,128)(2,1)S(1)} all-to-all(bf16[256,4,128]{0,2,1:T(8,128)(2,1)S(1)} %bitcast.100), channel_id=1, replica_groups=mesh['sp'=4,'fs'=4,'tp'=2] {'fs'}, dimensions={1} | all-to-all | bytes 524288 | tf_op jit(solution)/shard_map/all_to_all | solution.py:142
  15.4 0.9 copy.59
  16.4 1.5 fusion.8
  17.9 2.6 fusion.10
  20.6 0.1 copy.63
  20.7 7.9 %all_to_all.138 = bf16[256,4,128]{0,2,1:T(8,128)(2,1)S(1)} all-to-all(bf16[256,4,128]{0,2,1:T(8,128)(2,1)S(1)} %bitcast.101), channel_id=1, replica_groups=mesh['sp'=4,'fs'=4,'tp'=2] {'fs'}, dimensions={1} | all-to-all | bytes 524288 | tf_op jit(solution)/shard_map/all_to_all | solution.py:143
  28.7 0.8 copy.64
  29.6 0.1 copy.55
  29.7 8.1 %all_to_all.139 = bf16[256,4,128]{0,2,1:T(8,128)(2,1)S(1)} all-to-all(bf16[256,4,128]{0,2,1:T(8,128)(2,1)S(1)} %bitcast.102), channel_id=1, replica_groups=mesh['sp'=4,'fs'=4,'tp'=2] {'fs'}, dimensions={1} | all-to-all | bytes 524288 | tf_op jit(solution)/shard_map/all_to_all | solution.py:144
  37.8 0.8 copy.56
  38.7 0.8 copy.50
  39.6 5.6 %all-to-all-start = ((bf16[256,4,128]{0,2,1:T(8,128)(2,1)}), bf16[256,4,128]{0,2,1:T(8,128)(2,1)S(1)}, u32[]{:S(2)}, u32[]{:S(2)}) async-start(bf16[256,4,128]{0,2,1:T(8,128)(2,1)} %bitcast.2), calls=%async_computation | async-start | bytes 524288 | tf_op jit(solution)/shard_map/all_to_all | solution.py:141
  45.2 0.6 dynamic-slice.2
  46.5 0.3 multiply_cosine_fusion
  46.8 0.1 multiply_exponential_fusion.1
  47.0 1.9 all-to-all-done
  48.9 0.9 copy.51
  49.8 48.5 %all-gather.11.cloned.1.call-done = bf16[512,4096]{1,0:T(8,128)(2,1)} async-done(((bf16[128,4096]{1,0:T(8,128)(2,1)}), bf16[512,4096]{1,0:T(8,128)(2,1)}) %all-gather.11.cloned.1.call-update) | async-done | bytes 4194320 | tf_op jit(solution)/shard_map/all_gather | solution.py:139
  98.3 3.7 convolution_convert_fusion.1
  102.0 0.8 copy.60
  102.8 4.8 %all-to-all-start.5 = ((bf16[4,128,128]{1,2,0:T(8,128)(2,1)}), bf16[4,128,128]{1,2,0:T(8,128)(2,1)S(1)}, u32[]{:S(2)}, u32[]{:S(2)}) async-start(bf16[4,128,128]{1,2,0:T(8,128)(2,1)} %copy.60), calls=%async_computation.5 | async-start | bytes 262144 | tf_op jit(solution)/shard_map/all_to_all | solution.py:158
  107.5 19.7 %all-gather.19.cloned.1.call-done = bf16[4096,128]{1,0:T(8,128)(2,1)} async-done(((bf16[1024,128]{1,0:T(8,128)(2,1)}), bf16[4096,128]{1,0:T(8,128)(2,1)}) %all-gather.19.cloned.1.call-update) | async-done | bytes 1048592 | tf_op jit(solution)/shard_map/all_gather | solution.py:149
  127.2 3.7 convolution_convert_fusion
  131.0 0.8 copy.65
  131.7 4.2 all-to-all-start.7
  135.9 20.1 %all-gather.15.cloned.1.call-done = bf16[4096,128]{1,0:T(8,128)(2,1)} async-done(((bf16[1024,128]{1,0:T(8,128)(2,1)}), bf16[4096,128]{1,0:T(8,128)(2,1)}) %all-gather.15.cloned.1.call-update) | async-done | bytes 1048592 | tf_op jit(solution)/shard_map/all_gather | solution.py:150
  156.1 4.4 %convolution_convert_fusion.2 = bf16[512,128]{1,0:T(8,128)(2,1)} fusion(bf16[512,4096]{1,0:T(8,128)(2,1)} %all-gather.11.cloned.1.call-done, bf16[4096,128]{1,0:T(8,128)(2,1)} %all-gather.15.cloned.1.call-done), kind=kOutput, calls=%fused_computation.19 | convolution fusion | flops 536936448 | bytes 5373952 | tf_op jit(solution)/shard_map/dot_general | solution.py:153
  160.5 4.3 %all-to-all-start.3 = ((bf16[4,128,128]{2,1,0:T(8,128)(2,1)}), bf16[4,128,128]{2,1,0:T(8,128)(2,1)S(1)}, u32[]{:S(2)}, u32[]{:S(2)}) async-start(bf16[4,128,128]{2,1,0:T(8,128)(2,1)} %bitcast.22), calls=%async_computation.3 | async-start | bytes 262144 | tf_op jit(solution)/shard_map/all_to_all | solution.py:158
  165.3 2.3 all-to-all-done.3
  167.6 0.1 copy.57
  167.8 1.3 convolution_add_fusion
  169.2 0.7 all-gather.21.cloned.1.call-update
  169.9 0.7 all-gather.23.cloned.1.call-update
  170.6 9.3 %all-reduce = f32[8]{0:T(128)S(1)} all-reduce(f32[8]{0:T(128)S(1)} %get-tuple-element.181), channel_id=2, replica_groups=mesh['sp'=4,'fs'=4,'tp'=2] {'sp'}, use_global_device_ids=true, to_apply=%add | all-reduce | flops 8 | bytes 64
  180.2 0.6 fusion.53
  180.8 15.9 %all_gather.45 = f32[1,2,256,256]{3,2,1,0:T(8,128)S(1)} all-gather(f32[1,2,64,256]{3,2,1,0:T(8,128)S(1)} %copy-done.4), channel_id=1, replica_groups=mesh['sp'=4,'fs'=4,'tp'=2] {'sp'}, dimensions={2}, use_global_device_ids=true | all-gather | bytes 655360 | tf_op jit(solution)/shard_map/all_gather | solution.py:195
  196.7 3.9 convolution_convert_fusion.3
  200.7 0.8 copy.52
  201.5 7.0 %all-to-all-start.1 = ((bf16[4,128,128]{1,2,0:T(8,128)(2,1)}), bf16[4,128,128]{1,2,0:T(8,128)(2,1)S(1)}, u32[]{:S(2)}, u32[]{:S(2)}) async-start(bf16[4,128,128]{1,2,0:T(8,128)(2,1)} %copy.52), calls=%async_computation.1 | async-start | bytes 262144 | tf_op jit(solution)/shard_map/all_to_all | solution.py:158
  208.4 1.3 minimum_convert_fusion
  209.7 1.5 all-to-all-done.1
  211.3 0.1 slice.112
  211.4 1.5 collective-permute-start
  212.9 0.4 convolution_multiply_fusion
  213.3 0.3 fusion.54
  213.6 0.7 convolution_add_fusion.2
  214.3 4.7 %collective-permute-done = bf16[16,512]{1,0:T(8,128)(2,1)S(1)} collective-permute-done((bf16[16,512]{1,0:T(8,128)(2,1)S(1)}, bf16[16,512]{1,0:T(8,128)(2,1)S(1)}, u32[]{:S(2)}, u32[]{:S(2)}) %collective-permute-start) | collective-permute-done | bytes 16416 | tf_op jit(solution)/shard_map/ppermute | solution.py:24
  219.0 0.1 copy.54
  219.1 0.1 maximum_convert_fusion
  219.3 1.1 fusion.14
  220.6 0.3 fusion.27
  220.8 0.3 fusion.25
  221.2 11.8 %all-gather.25.cloned.1.call-done = f32[8,256,256]{2,1,0:T(8,128)} async-done(((f32[2,256,256]{2,1,0:T(8,128)}), f32[8,256,256]{2,1,0:T(8,128)}) %all-gather.25.cloned.1.call-update) | async-done | bytes 2097168 | tf_op jit(solution)/shard_map/all_gather | solution.py:29
  233.0 3.6 while.9
  233.0 1.2 fusion.67
  234.2 1.2 fusion.67
  235.4 1.2 fusion.67
  236.6 1.2 multiply_reduce_fusion
  237.8 0.1 copy.76
  237.9 82.6 %all-gather.21.cloned.1.call-done = bf16[512,4096]{1,0:T(8,128)(2,1)} async-done(((bf16[512,256]{1,0:T(8,128)(2,1)}), bf16[512,4096]{1,0:T(8,128)(2,1)}) %all-gather.21.cloned.1.call-update) | async-done | bytes 4194320 | tf_op jit(solution)/shard_map/all_gather | solution.py:211
  320.6 87.7 %all-gather.23.cloned.1.call-done = bf16[512,4096]{1,0:T(8,128)(2,1)} async-done(((bf16[512,256]{1,0:T(8,128)(2,1)}), bf16[512,4096]{1,0:T(8,128)(2,1)}) %all-gather.23.cloned.1.call-update) | async-done | bytes 4194320 | tf_op jit(solution)/shard_map/all_gather | solution.py:212
  408.3 5.8 %fusion.5 = bf16[128,4096]{1,0:T(8,128)(2,1)} fusion(bf16[512,4096]{1,0:T(8,128)(2,1)} %all-gather.23.cloned.1.call-done, bf16[512,4096]{1,0:T(8,128)(2,1)} %all-gather.21.cloned.1.call-done, bf16[128,512]{1,0:T(8,128)(2,1)S(1)} %copy.76, bf16[128,512]{1,0:T(8,128)(2,1)S(1)} %fusion.15), kind=kOutput, calls=%fused_computation.7 | convolution fusion | flops 1091567616 | bytes 9699328 | tf_op jit(solution)/shard_map/dot_general | solution.py:217
  414.1 9.9 %reduce-scatter.2.cloned.1.call-done = bf16[64,4096]{1,0:T(8,128)(2,1)} async-done(((bf16[128,4096]{1,0:T(8,128)(2,1)}), bf16[64,4096]{1,0:T(8,128)(2,1)}) %reduce-scatter.2.cloned.1.call-update) | async-done | bytes 524304 | tf_op jit(solution)/shard_map/reduce_scatter | solution.py:216
  (68 shorter events, 1.6 us)
Async XLA Ops:
  6.5 214.0 %copy-start = (bf16[4,256,256]{2,1,0:T(8,128)(2,1)S(1)}, bf16[4,256,256]{2,1,0:T(8,128)(2,1)}, u32[]{:S(2)}) copy-start(bf16[4,256,256]{2,1,0:T(8,128)(2,1)} %param.23) | copy-start | bytes 1572868
  6.5 14.1 %copy-start.1 = (bf16[256,512]{1,0:T(8,128)(2,1)S(1)}, bf16[256,512]{1,0:T(8,128)(2,1)}, u32[]{:S(2)}) copy-start(bf16[256,512]{1,0:T(8,128)(2,1)} %param.21) | copy-start | bytes 786436
  6.5 23.0 %copy-start.2 = (bf16[256,512]{1,0:T(8,128)(2,1)S(1)}, bf16[256,512]{1,0:T(8,128)(2,1)}, u32[]{:S(2)}) copy-start(bf16[256,512]{1,0:T(8,128)(2,1)} %param.22) | copy-start | bytes 786436
  6.5 43.2 %all-gather.17.cloned.1.call-start = ((), (), s32[]{:S(2)}) async-start(), calls=%async_computation.12 | async-start | bytes 1310720 | tf_op jit(solution)/shard_map/all_gather | solution.py:148
  16.3 22.4 %copy-start.3 = (bf16[256,512]{1,0:T(8,128)(2,1)S(1)}, bf16[256,512]{1,0:T(8,128)(2,1)}, u32[]{:S(2)}) copy-start(bf16[256,512]{1,0:T(8,128)(2,1)} %param.19) | copy-start | bytes 786436
  16.3 81.9 %all-gather.11.cloned.1.call-start = ((), (), s32[]{:S(2)}) async-start(), calls=%async_computation.9 | async-start | bytes 5242880 | tf_op jit(solution)/shard_map/all_gather | solution.py:139
  17.9 27.3 %copy-start.8 = (u32[32]{0:T(128)S(1)}, u32[32]{0:T(128)}, u32[]{:S(2)}) copy-start(u32[32]{0:T(128)} %constant.104) | copy-start | bytes 388
  17.9 28.5 %copy-start.5 = (f32[2]{0:T(128)S(1)}, f32[2]{0:T(128)}, u32[]{:S(2)}) copy-start(f32[2]{0:T(128)} %param.25) | copy-start | bytes 28
  20.5 106.7 %all-gather.19.cloned.1.call-start = ((), (), s32[]{:S(2)}) async-start(), calls=%async_computation.13 | async-start | bytes 1310720 | tf_op jit(solution)/shard_map/all_gather | solution.py:149
  29.5 126.5 %all-gather.15.cloned.1.call-start = ((), (), s32[]{:S(2)}) async-start(), calls=%async_computation.11 | async-start | bytes 1310720 | tf_op jit(solution)/shard_map/all_gather | solution.py:150
  39.6 9.3 %all-to-all-start = ((bf16[256,4,128]{0,2,1:T(8,128)(2,1)}), bf16[256,4,128]{0,2,1:T(8,128)(2,1)S(1)}, u32[]{:S(2)}, u32[]{:S(2)}) async-start(bf16[256,4,128]{0,2,1:T(8,128)(2,1)} %bitcast.2), calls=%async_computation | async-start | bytes 524288 | tf_op jit(solution)/shard_map/all_to_all | solution.py:141
  45.1 151.6 %all-gather.13.cloned.1.call-start = ((), (), s32[]{:S(2)}) async-start(), calls=%async_computation.10 | async-start | bytes 1310720 | tf_op jit(solution)/shard_map/all_gather | solution.py:147
  102.8 29.0 %all-to-all-start.5 = ((bf16[4,128,128]{1,2,0:T(8,128)(2,1)}), bf16[4,128,128]{1,2,0:T(8,128)(2,1)S(1)}, u32[]{:S(2)}, u32[]{:S(2)}) async-start(bf16[4,128,128]{1,2,0:T(8,128)(2,1)} %copy.60), calls=%async_computation.5 | async-start | bytes 262144 | tf_op jit(solution)/shard_map/all_to_all | solution.py:158
  131.7 28.7 %all-to-all-start.7 = ((bf16[4,128,128]{1,2,0:T(8,128)(2,1)}), bf16[4,128,128]{1,2,0:T(8,128)(2,1)S(1)}, u32[]{:S(2)}, u32[]{:S(2)}) async-start(bf16[4,128,128]{1,2,0:T(8,128)(2,1)} %copy.65), calls=%async_computation.7 | async-start | bytes 262144 | tf_op jit(solution)/shard_map/all_to_all | solution.py:158
  160.4 19.6 %copy-start.7 = (f32[1024]{0:T(1024)S(1)}, f32[1024]{0:T(1024)}, u32[]{:S(2)}) copy-start(f32[1024]{0:T(1024)} %param.24) | copy-start | bytes 12292
  160.4 19.7 %copy-start.6 = (s32[4]{0:T(128)S(1)}, s32[4]{0:T(128)}, u32[]{:S(2)}) copy-start(s32[4]{0:T(128)} %constant.99.clone) | copy-start | bytes 52
  160.4 20.4 %copy-start.4 = (f32[1,2,64,256]{3,2,1,0:T(8,128)S(1)}, f32[1,2,64,256]{3,2,1,0:T(8,128)}, u32[]{:S(2)}) copy-start(f32[1,2,64,256]{3,2,1,0:T(8,128)} %param.26) | copy-start | bytes 393220
  160.5 7.1 %all-to-all-start.3 = ((bf16[4,128,128]{2,1,0:T(8,128)(2,1)}), bf16[4,128,128]{2,1,0:T(8,128)(2,1)S(1)}, u32[]{:S(2)}, u32[]{:S(2)}) async-start(bf16[4,128,128]{2,1,0:T(8,128)(2,1)} %bitcast.22), calls=%async_computation.3 | async-start | bytes 262144 | tf_op jit(solution)/shard_map/all_to_all | solution.py:158
  164.8 68.1 %all-gather.25.cloned.1.call-start = ((), (), s32[]{:S(2)}) async-start(), calls=%async_computation.17 | async-start | bytes 2621440 | tf_op jit(solution)/shard_map/all_gather | solution.py:29
  169.1 151.4 %all-gather.21.cloned.1.call-start = ((), (), s32[]{:S(2)}) async-start(), calls=%async_computation.14 | async-start | bytes 4456448 | tf_op jit(solution)/shard_map/all_gather | solution.py:211
  169.9 238.4 %all-gather.23.cloned.1.call-start = ((), (), s32[]{:S(2)}) async-start(), calls=%async_computation.15 | async-start | bytes 4456448 | tf_op jit(solution)/shard_map/all_gather | solution.py:212
  201.5 9.8 %all-to-all-start.1 = ((bf16[4,128,128]{1,2,0:T(8,128)(2,1)}), bf16[4,128,128]{1,2,0:T(8,128)(2,1)S(1)}, u32[]{:S(2)}, u32[]{:S(2)}) async-start(bf16[4,128,128]{1,2,0:T(8,128)(2,1)} %copy.52), calls=%async_computation.1 | async-start | bytes 262144 | tf_op jit(solution)/shard_map/all_to_all | solution.py:158
  208.4 215.5 %reduce-scatter.2.cloned.1.call-start = ((), (), s32[]{:S(2)}) async-start(), calls=%async_computation.16 | async-start | bytes 1572864 | tf_op jit(solution)/shard_map/reduce_scatter | solution.py:216
  211.4 7.6 %collective-permute-start = (bf16[16,512]{1,0:T(8,128)(2,1)S(1)}, bf16[16,512]{1,0:T(8,128)(2,1)S(1)}, u32[]{:S(2)}, u32[]{:S(2)}) collective-permute-start(bf16[16,512]{1,0:T(8,128)(2,1)S(1)} %copy.75), channel_id=1, source_target_pairs={{0,8},{8,16},{16,24},{1,9},{9,17},{17,25},{2,10},{10,18},{18,26},{... | collective-permute-start | bytes 49160 | tf_op jit(solution)/shard_map/ppermute | solution.py:24
Sparse Core Ops, SparseCore 0:
  16.4 27.3 all-gather.16
  45.7 52.5 all-gather.10
  99.8 27.3 all-gather.18
  128.7 27.3 all-gather.14
  157.5 29.2 all-gather.12
  188.2 44.7 all-gather.24
  235.7 84.8 all-gather.20
  323.3 84.9 all-gather.22
  414.2 9.7 reduce-scatter.1
where the time goes:
time: 433 us; the launch traced here: 430 us
  waiting for transfers between devices  292 us (67%)
  blocking collectives  49 us (11%)
  starting transfers between devices  27.5 us (6%)
  matrix products  26 us (6%)
  between operations  14.1 us (3%)
  other arithmetic  11.1 us (3%)
  local copies, waits for them, and re-layouts  10.4 us (2%)
    all_gather x1, waiting for transfers between devices, on_device(): lax.all_gather(retention_back, ('sp', 'fs'), axis=1, tiled=True)  87.7 us
    all_gather x1, waiting for transfers between devices, on_device(): lax.all_gather(pool_back, ('sp', 'fs'), axis=1, tiled=True)  82.6 us
    all_gather x1, waiting for transfers between devices, on_device(): group_normed = lax.all_gather(normed, 'fs', axis=0, tiled=True)  48.5 us
    all_to_all x4, starting transfers between devices, on_device(): lax.all_to_all(shortened(rounded), 'fs', split_axis=0, concat_axis=1, til...  20.3 us
    all_gather x1, waiting for transfers between devices, on_device(): lax.all_gather(quarters[3], 'sp', axis=0, tiled=True)  20.1 us
    all_gather x1, waiting for transfers between devices, on_device(): lax.all_gather(quarters[2], 'sp', axis=0, tiled=True)  19.7 us
    all_gather x1, blocking collectives, on_device(): whole_start = lax.all_gather(start_state, 'sp', axis=2, tiled=True)[0]  15.9 us
    dot_general x4, matrix products, on_device(): jnp.dot(group_normed, piece_w, preferred_element_type=jnp.float32)  15.8 us
  transfers between devices with their start and end apart: 15, of which 11 were waited for; matrix products, arithmetic and copies ran while one was open for 9% of the time, Pallas kernels for 0%

commit v1 on v0

--- a/solution.py
+++ b/solution.py
@@ -1,3 +1,8 @@
+import functools
+
+from jax.experimental import pallas as pl
+from jax.experimental.pallas import tpu as pltpu
+
 import jax
 import jax.numpy as jnp
 from jax import lax
@@ -222,7 +227,369 @@
     return mixed[None]
 
 
+MESH = pl.DeviceIdType.MESH
+
+
+def where_am_i():
+    sp, fs, tp = (lax.axis_index(name) for name in ("sp", "fs", "tp"))
+    return sp, fs, tp, fs // 2, fs % 2
+
+
+def remote(src, dst, send, recv, target):
+    return pltpu.make_async_remote_copy(
+        src_ref=src, dst_ref=dst, send_sem=send, recv_sem=recv, device_id=target, device_id_type=MESH
+    )
+
+
+def cols(index, size):
+    return pl.ds(pl.multiple_of(index * size, size), size)
+
+
+def project_kernel(
+    tok, gain, wp, wq, wk, wv, state, pb, rb,
+    joined, start, backs,
+    xn, xg, wg, part, got,
+    w_send, w_recv, w_local, x_send, x_recv, x_local, f_send, f_recv,
+    s_send, s_recv, b_send, b_recv, b_local, p_send, p_recv, j_send, j_recv,
+):
+    sp, fs, tp, y, x = where_am_i()
+    nsp, nfs = 4, 4
+    span, width = tok.shape
+    half = span // 2
+    feats = width // nsp
+    rows, group = wg.shape[2], wg.shape[3]
+    mats = (wp, wq, wk, wv)
+    partner = (sp, fs, 1 - tp)
+    waits = []
+
+    for d in range(1, nfs):
+        to = lax.rem(fs + d, nfs)
+        for m, mat in enumerate(mats):
+            c = remote(
+                mat.at[:, cols(to // 2, group)], wg.at[fs, m], w_send.at[d - 1, m],
+                w_recv.at[fs, m], (sp, to, tp),
+            )
+            c.start()
+            waits.append(c)
+    own_w = []
+    for m, mat in enumerate(mats):
+        c = pltpu.make_async_copy(mat.at[:, cols(y, group)], wg.at[fs, m], w_local.at[m])
+        c.start()
+        own_w.append(c)
+    for j in range(2):
+        for h in range(2):
+            to_sp, to_fs = 2 * y + tp, 2 * j + x
+            rs = state.shape[1]
+            dst = start.at[pl.ds(pl.multiple_of(sp * rs, rs), rs)]
+            same = (to_sp == sp) & (to_fs == fs) & (tp == h)
+
+            @pl.when(same)
+            def _():
+                pltpu.make_async_copy(state.at[j], dst, s_recv.at[sp]).start()
+
+            @pl.when(jnp.logical_not(same))
+            def _():
+                remote(state.at[j], dst, s_send.at[2 * j + h], s_recv.at[sp], (to_sp, to_fs, h)).start()
+
+    floats = tok[...].astype(jnp.float32)
+    xn[...] = (
+        floats * lax.rsqrt(jnp.mean(floats * floats, axis=-1, keepdims=True) + eps) * gain[...]
+    ).astype(jnp.bfloat16)
+
+    mine = pl.ds(pl.multiple_of(tp * half, half), half)
+    moves = [(dz, dy) for dz in range(nsp) for dy in range(2) if dz or dy]
+    for i, (dz, dy) in enumerate(moves):
+        to_sp, to_y = lax.rem(sp + dz, nsp), lax.rem(y + dy, 2)
+        c = remote(
+            xn.at[mine, cols(to_sp, feats)], xg.at[y, sp, mine], x_send.at[i],
+            x_recv.at[y, sp], (to_sp, 2 * to_y + x, tp),
+        )
+        c.start()
+        waits.append(c)
+    own_x = pltpu.make_async_copy(xn.at[:, cols(sp, feats)], xg.at[y, sp], x_local)
+    own_x.start()
+
+    forwards = []
+    for i, (dz, dy) in enumerate(moves):
+        fr_sp, fr_y = lax.rem(sp + nsp - dz, nsp), lax.rem(y + dy, 2)
+        slot = xg.at[fr_y, fr_sp, mine]
+        remote(slot, slot, x_send.at[i], x_recv.at[fr_y, fr_sp], partner).wait_recv()
+        c = remote(slot, slot, f_send.at[i], f_recv.at[i], partner)
+        c.start()
+        forwards.append(c)
+
+    own_b = []
+    for b, back in enumerate((pb, rb)):
+        c = pltpu.make_async_copy(back, backs.at[fs, b], b_local.at[b])
+        c.start()
+        own_b.append(c)
+        for d in range(1, nfs):
+            to = lax.rem(fs + d, nfs)
+            c = remote(back, backs.at[fs, b], b_send.at[d - 1, b], b_recv.at[fs, b], (sp, to, tp))
+            c.start()
+            waits.append(c)
+
+    own_x.wait()
+    for c in own_w:
+        c.wait()
+    for c in forwards:
+        c.wait()
+    for d in range(1, nfs):
+        fr = lax.rem(fs + nfs - d, nfs)
+        for m, mat in enumerate(mats):
+            remote(
+                mat.at[:, cols(y, group)], wg.at[fr, m], w_send.at[d - 1, m], w_recv.at[fr, m], partner
+            ).wait_recv()
+
+    tall = 2 * span
+    for s in range(2):
+        for h in range(2):
+            for m in range(4):
+                acc = jnp.zeros((tall, group), jnp.float32)
+                for f in range(nfs):
+                    lhs = jnp.concatenate(
+                        [xg[s, 2 * h + k, :, f * rows : (f + 1) * rows] for k in range(2)], axis=0
+                    )
+                    acc += jnp.dot(lhs, wg[f, m], preferred_element_type=jnp.float32)
+                part[s, h, :, m * group : (m + 1) * group] = acc.astype(jnp.bfloat16)
+            same = (2 * s + tp == sp) & (tp == h)
+
+            @pl.when(same)
+            def _():
+                pltpu.make_async_copy(part.at[s, h], got.at[sp], p_recv.at[sp]).start()
+
+            @pl.when(jnp.logical_not(same))
+            def _():
+                remote(
+                    part.at[s, h], got.at[sp], p_send.at[2 * s + h], p_recv.at[sp], (2 * s + tp, fs, h)
+                ).start()
+
+    for k in range(nsp):
+        remote(part.at[0, 0], got.at[k], p_send.at[0], p_recv.at[k], partner).wait_recv()
+    total = got[0].astype(jnp.float32)
+    for k in range(1, nsp):
+        total += got[k].astype(jnp.float32)
+    joined[tp] = total.astype(jnp.bfloat16)
+    last = remote(joined.at[tp], joined.at[tp], j_send, j_recv, partner)
+    last.start()
+    last.wait_send()
+    remote(joined.at[1 - tp], joined.at[1 - tp], j_send, j_recv, partner).wait_recv()
+
+    for j in range(2):
+        for h in range(2):
+            to_sp, to_fs = 2 * y + tp, 2 * j + x
+            same = (to_sp == sp) & (to_fs == fs) & (tp == h)
+
+            @pl.when(jnp.logical_not(same))
+            def _():
+                remote(state.at[j], start.at[pl.ds(0, state.shape[1])], s_send.at[2 * j + h], s_recv.at[0], partner).wait_send()
+
+            same_p = (2 * j + tp == sp) & (tp == h)
+
+            @pl.when(jnp.logical_not(same_p))
+            def _():
+                remote(part.at[j, h], got.at[0], p_send.at[2 * j + h], p_recv.at[0], partner).wait_send()
+
+    for k in range(nsp):
+        rs = state.shape[1]
+        slot = start.at[k * rs : (k + 1) * rs]
+        remote(slot, slot, s_send.at[0], s_recv.at[k], partner).wait_recv()
+    for b, back in enumerate((pb, rb)):
+        own_b[b].wait()
+        for d in range(1, nfs):
+            fr = lax.rem(fs + nfs - d, nfs)
+            remote(back, backs.at[fr, b], b_send.at[d - 1, b], b_recv.at[fr, b], partner).wait_recv()
+    for c in waits:
+        c.wait_send()
+
+
+def output_kernel(
+    yh, backs, out,
+    yg, accs, give, take, done,
+    y_send, y_recv, g_send, g_recv, o_send, o_recv, o_local,
+):
+    sp, fs, tp, y, x = where_am_i()
+    nsp, nfs = 4, 4
+    half, wide = yh.shape
+    group = wide // 2
+    block = backs.shape[3]
+    few = out.shape[0]
+    across = nfs * block
+    partner = (sp, fs, 1 - tp)
+    s, p = sp // 2, sp % 2
+    for k in range(nsp):
+        same = (sp == k) & (s == y) & (p == tp)
+
+        @pl.when(same)
+        def _():
+            pltpu.make_async_copy(yh, yg.at[y, tp], y_recv.at[y, tp]).start()
+
+        @pl.when(jnp.logical_not(same))
+        def _():
+            remote(yh, yg.at[y, tp], y_send.at[k], y_recv.at[y, tp], (k, 2 * s + x, p)).start()
+
+    gives = []
+    for h in range(2):
+        for q in range(2):
+            remote(yh, yg.at[q, h], y_send.at[0], y_recv.at[q, h], partner).wait_recv()
+        for f in range(nfs):
+            acc = jnp.zeros((half, block), jnp.float32)
+            for q in range(2):
+                for b in range(2):
+                    acc += jnp.dot(
+                        yg[q, h, :, b * group : (b + 1) * group],
+                        backs[f, b, q * group : (q + 1) * group, :],
+                        preferred_element_type=jnp.float32,
+                    )
+            accs[h * half : (h + 1) * half, f * block : (f + 1) * block] = acc
+        for k in (2 * h, 2 * h + 1):
+            off = pl.multiple_of(k * 2 * few + (1 - tp) * few, few)
+            give[k] = accs[pl.ds(off, few), :].astype(jnp.bfloat16)
+            c = remote(give.at[k], take.at[k], g_send.at[k], g_recv.at[k], partner)
+            c.start()
+            gives.append(c)
+    for k in range(nsp):
+        gives[k].wait()
+        off = pl.multiple_of(k * 2 * few + tp * few, few)
+        done[k] = (accs[pl.ds(off, few), :] + take[k].astype(jnp.float32)).astype(jnp.bfloat16)
+        dst = out.at[:, cols(sp, across)]
+
+        @pl.when(sp == k)
+        def _():
+            pltpu.make_async_copy(done.at[k], dst, o_recv.at[sp]).start()
+
+        @pl.when(sp != k)
+        def _():
+            remote(done.at[k], dst, o_send.at[k], o_recv.at[sp], (k, fs, tp)).start()
+
+    for k in range(nsp):
+        remote(done.at[k], out.at[:, k * across : (k + 1) * across], o_send.at[k], o_recv.at[k], partner).wait_recv()
+
+        @pl.when(sp != k)
+        def _():
+            remote(done.at[k], out.at[:, k * across : (k + 1) * across], o_send.at[k], o_recv.at[k], partner).wait_send()
+
+        same = (sp == k) & (s == y) & (p == tp)
+
+        @pl.when(jnp.logical_not(same))
+        def _():
+            remote(yh, yg.at[0, 0], y_send.at[k], y_recv.at[0, 0], partner).wait_send()
+
+
+def turned(values, cosine, sine):
+    half_dim = values.shape[-1] // 2
+    a, b = values[:, :half_dim], values[:, half_dim:]
+    return jnp.concatenate([a * cosine - b * sine, a * sine + b * cosine], axis=-1)
+
+
+def angles_of(positions, half_dim):
+    inv_freq = 1.0 / rope_base ** jnp.linspace(0.0, 1.0, half_dim, dtype=jnp.float32)
+    angles = positions.astype(jnp.float32)[:, None] * inv_freq[None, :]
+    return jnp.cos(angles), jnp.sin(angles)
+
+
+def paired(
+    tokens, norm_gain, pool_proj, query_proj, key_proj, value_proj, pool_map, pool_scale,
+    decay_rate, start_state, pool_back, retention_back,
+):
+    bf, f32 = jnp.bfloat16, jnp.float32
+    sp, fs, tp, y, x = where_am_i()
+    nsp = lax.axis_size("sp")
+    tok = tokens[0]
+    span, width = tok.shape
+    rows, two = pool_proj.shape
+    group = two // 2
+    length = nsp * span
+    half = length // 2
+    vm, hbm = pl.BlockSpec(memory_space=pltpu.VMEM), pl.BlockSpec(memory_space=pl.ANY)
+    dma = pltpu.SemaphoreType.DMA
+    rs = start_state.shape[2]
+    joined, start, backs = pl.pallas_call(
+        project_kernel,
+        out_shape=(
+            jax.ShapeDtypeStruct((2, half, 4 * group), bf),
+            jax.ShapeDtypeStruct((nsp * rs, group), bf),
+            jax.ShapeDtypeStruct((4, 2) + pool_back.shape, bf),
+        ),
+        in_specs=[vm, vm, hbm, hbm, hbm, hbm, hbm, hbm, hbm],
+        out_specs=(vm, vm, vm),
+        scratch_shapes=[
+            pltpu.VMEM((span, width), bf),
+            pltpu.VMEM((2, nsp, span, width // nsp), bf),
+            pltpu.VMEM((4, 4, rows, group), bf),
+            pltpu.VMEM((2, 2, half, 4 * group), bf),
+            pltpu.VMEM((nsp, half, 4 * group), bf),
+            dma((3, 4)), dma((4, 4)), dma((4,)), dma((7,)), dma((2, nsp)), dma,
+            dma((7,)), dma((7,)), dma((4,)), dma((nsp,)), dma((3, 2)), dma((4, 2)), dma((2,)),
+            dma((4,)), dma((nsp,)), dma, dma,
+        ],
+        compiler_params=pltpu.CompilerParams(has_side_effects=True, vmem_limit_bytes=48 * 2**20),
+        name="project",
+    )(
+        tok, norm_gain[None, :], pool_proj, query_proj, key_proj, value_proj,
+        start_state[0].astype(bf), pool_back, retention_back,
+    )
+    whole = joined.reshape(length, 4 * group)
+    mine = joined[tp] if False else lax.dynamic_index_in_dim(joined, tp, 0, keepdims=False)
+    head = 2 * (sp % 2) + y
+    local = lax.dynamic_index_in_dim(decay_rate, y, 0, keepdims=False)
+    other = lax.ppermute(decay_rate, "tp", [(0, 1), (1, 0)])
+    rate = jnp.where(sp % 2 == tp, local, lax.dynamic_index_in_dim(other, y, 0, keepdims=False))
+    every = jnp.arange(length, dtype=jnp.int32)
+    position = tp * half + jnp.arange(half, dtype=jnp.int32)
+
+    pool_all = jnp.concatenate([jnp.zeros((HALO, group), f32), whole[:, :group].astype(f32)], axis=0)
+    extended = lax.dynamic_slice_in_dim(pool_all, tp * half, half + HALO, 0)
+    sums = trailing_sums(extended, half)
+    windows = jnp.array(window_list, dtype=jnp.int32)
+    chosen = sums[0]
+    for i in range(1, GROUPS):
+        chosen = jnp.where(head == i, sums[i], chosen)
+    counts = jnp.minimum(windows[head], position + 1).astype(f32)
+    differ = (chosen / counts[:, None] - extended[HALO:]).astype(bf)
+    this_map = lax.dynamic_index_in_dim(pool_map, head, 0, keepdims=False)
+    scale = lax.dynamic_slice_in_dim(pool_scale, head * group, group, 0)
+    pool_out = (jnp.dot(differ, this_map, preferred_element_type=f32) * scale).astype(bf)
+
+    cosine, sine = angles_of(every, group // 2)
+    my_cos = lax.dynamic_slice_in_dim(cosine, tp * half, half, 0)
+    my_sin = lax.dynamic_slice_in_dim(sine, tp * half, half, 0)
+    rq = turned(mine[:, group : 2 * group].astype(f32), my_cos, my_sin)
+    rk = turned(whole[:, 2 * group : 3 * group].astype(f32), cosine, sine) * group ** (-0.5)
+    value = whole[:, 3 * group :].astype(f32)
+    gap = (position[:, None] - every[None, :]).astype(f32)
+    mask = jnp.where(gap >= 0, jnp.exp(-jnp.maximum(gap, 0.0) * rate), 0.0)
+    high = lax.Precision.HIGHEST
+    scores = jnp.dot(rq, rk.T, precision=high) * mask
+    fade = jnp.exp(-(position.astype(f32) + 1.0) * rate)
+    ret = jnp.dot(scores, value, precision=high) + jnp.dot(
+        rq * fade[:, None], start.astype(f32), precision=high
+    )
+    ret = ret * lax.rsqrt(jnp.mean(ret * ret, axis=-1, keepdims=True) + eps)
+    yh = jnp.concatenate([pool_out, ret.astype(bf)], axis=1)
+
+    few = span // 2
+    return pl.pallas_call(
+        output_kernel,
+        out_shape=jax.ShapeDtypeStruct((few, width), bf),
+        in_specs=[vm, vm],
+        out_specs=vm,
+        scratch_shapes=[
+            pltpu.VMEM((2, 2, half, 2 * group), bf),
+            pltpu.VMEM((length, 4 * pool_back.shape[1]), f32),
+            pltpu.VMEM((nsp, few, 4 * pool_back.shape[1]), bf),
+            pltpu.VMEM((nsp, few, 4 * pool_back.shape[1]), bf),
+            pltpu.VMEM((nsp, few, 4 * pool_back.shape[1]), bf),
+            dma((nsp,)), dma((2, 2)), dma((nsp,)), dma((nsp,)), dma((nsp,)), dma((nsp,)), dma,
+        ],
+        compiler_params=pltpu.CompilerParams(has_side_effects=True, vmem_limit_bytes=48 * 2**20),
+        name="output",
+    )(yh, backs)[None]
+
+
 def solution(mesh):
+    sizes = mesh.shape
+    small = sizes["sp"] == 4 and sizes["fs"] == 4 and sizes["tp"] == 2
     placed = (
         P("fs", "sp", None),
         P(),
@@ -238,7 +605,7 @@
         P("tp", ("sp", "fs")),
     )
     return jax.shard_map(
-        on_device,
+        paired if small else on_device,
         mesh=mesh,
         in_specs=placed,
         out_specs=P("fs", ("sp", "tp"), None),

time: 433 us -> 173 us (0.40)
  waiting for transfers between devices: 292 us -> 0.01 us
  Pallas kernels: 0 us -> 148 us
  blocking collectives: 49 us -> 0 us
  starting transfers between devices: 27.5 us -> 0.01 us
  matrix products: 26 us -> 3.67 us
  between operations: 14.1 us -> 1.47 us
  other arithmetic: 11.1 us -> 5.63 us
    all_gather x8 -> x0, waiting for transfers between devices: 270 us -> none  [the longest x1 87.7 us: on_device(): lax.all_gather(retention_back, ('sp', 'fs'), axis=1, tiled=True)]
    pallas_call x0 -> x2, Pallas kernels: none -> 148 us  [the longest x1 96.8 us: paired(): pl.pallas_call(project_kernel, out_shape=(jax.ShapeDtypeStruct((2, half,...]
    all_to_all x5 -> x0, starting transfers between devices: 25.9 us -> none  [the longest x4 20.3 us: on_device(): lax.all_to_all(shortened(rounded), 'fs', split_axis=0, concat_axis=1, til...]
    all_to_all x3 -> x0, blocking collectives: 23.7 us -> none  [the longest x1 8.11 us: on_device(): lax.all_to_all(value_proj, 'fs', split_axis=1, concat_axis=0, tiled=True)]
    dot_general x12 -> x4, matrix products: 26 us -> 3.67 us  [the longest x1 1.34 us: paired(): jnp.dot(scores, value, precision=high)]
    all_gather x1 -> x0, blocking collectives: 15.9 us -> none  [on_device(): whole_start = lax.all_gather(start_state, 'sp', axis=2, tiled=True)[0]]
    reduce_scatter x1 -> x0, waiting for transfers between devices: 9.87 us -> none  [on_device(): lax.psum_scatter(jnp.dot(joined, weight_local, preferred_element_type=jnp...]
    unnamed x1 -> x0, blocking collectives: 9.35 us -> none
  transfers between devices with their start and end apart: 15 -> 1, of which waited for: 11 -> 0; matrix products, arithmetic and copies ran while one was open for 9% -> 6% of each run, Pallas kernels for 0% -> 57%
where the time goes in v1:
time: 173 us; the launch traced here: 171 us
  Pallas kernels  148 us (86%)
  local copies, waits for them, and re-layouts  12.6 us (7%)
  other arithmetic  5.63 us (3%)
  matrix products  3.67 us (2%)
    pallas_call x1, Pallas kernels, paired(): pl.pallas_call(project_kernel, out_shape=(jax.ShapeDtypeStruct((2, half,...  96.8 us
    pallas_call x1, Pallas kernels, paired(): pl.pallas_call(output_kernel, out_shape=jax.ShapeDtypeStruct((few, width)...  50.8 us
    unnamed x27, local copies, waits for them, and re-layouts  8.65 us
  transfers between devices with their start and end apart: 1, of which 0 were waited for; matrix products, arithmetic and copies ran while one was open for 6% of the time, Pallas kernels for 57%

profile of v1, /device:TPU:30, one launch (start us, length us, event | category | flops | bytes accessed | tf_op | source)
XLA Modules:
  0.0 170.9 jit_solution(17248583944762788365)
XLA Ops:
  0.0 0.0 copy-start
  0.0 0.0 collective-permute-start
  0.1 0.5 multiply_add_fusion.2
  0.6 1.3 dynamic_slice.37
  1.8 1.2 dynamic_slice.31
  3.0 0.5 minimum_convert_fusion
  3.6 0.9 convert_bitcast_fusion.state
  4.5 0.0 copy-start.2
  4.5 1.2 copy-done.2
  5.7 0.0 copy-start.3
  5.7 0.9 copy-done.3
  6.7 0.0 copy-start.4
  6.7 0.9 copy-done.4
  7.6 0.0 copy-start.5
  7.6 0.9 copy-done.5
  8.6 0.0 copy-start.6
  8.6 0.9 copy-done.6
  9.5 0.0 copy-start.7
  9.5 0.9 copy-done.7
  10.5 0.0 copy-start.8
  10.5 0.9 copy-done.8
  11.4 0.0 copy-start.9
  11.4 0.7 copy-done.9
  12.2 96.8 %project.1 = (bf16[2,256,1024]{2,1,0:T(8,128)(2,1)S(1)}, bf16[256,256]{1,0:T(8,128)(2,1)S(1)}, bf16[4,2,512,256]{3,2,1,0:T(8,128)(2,1)S(1)}) custom-call(bf16[128,4096]{1,0:T(8,128)(2,1)S(1)} %bitcast.19, f32[1,4096]{1,0:T(1,128)S(1)} %bitcast.20, bf16[256,512]{1,0:T(8,128)(2,1)S(1)} %copy-done.3, bf16[256,512]{1,0:T(8,128)(2,1)S(1)} %copy-done.4, ...), custom_call_target="tpu_custom_call" | custom-call | tf_op jit(solution)/shard_map/project/pallas_call | solution.py:507
  108.9 0.0 copy-start.1
  109.0 0.8 slice_convert_fusion.1
  109.8 0.2 copy-done.1
  110.0 0.1 fusion.21
  110.1 0.0 copy-start.10
  110.1 0.8 dynamic_slice.33
  110.9 0.7 fusion.17
  111.6 1.8 %multiply_cosine_fusion = (f32[512,128]{1,0:T(8,128)S(1)}, f32[512,128]{1,0:T(8,128)S(1)}, f32[512,128]{1,0:T(8,128)S(1)}, f32[512,128]{1,0:T(8,128)}) fusion(f32[128]{0:T(128)S(1)} %fusion.17, f32[512]{0:T(512)S(1)} %iota_convert_fusion, f32[512,256]{1,0:T(8,128)S(1)} %get-tuple-element.12), kind=kLoop, calls=%fused_computation.10 | loop fusion | flops 458752 | bytes 1575424 | tf_op jit(solution)/shard_map/cos | solution.py:488
  113.5 0.0 copy-done.10
  113.5 0.0 copy-done
  113.5 0.0 copy-start.11
  113.5 1.2 fusion
  114.7 0.0 collective-permute-done
  114.7 0.6 dynamic_slice.38
  116.6 0.0 copy-done.11
  116.6 0.0 copy-start.12
  116.6 0.7 convolution_multiply_fusion
  117.4 1.3 fusion.3
  118.7 0.4 multiply_reduce_fusion
  119.1 0.1 multiply_convert_fusion
  119.2 0.0 copy-done.12
  119.3 50.8 %output.1 = bf16[64,4096]{1,0:T(8,128)(2,1)S(1)} custom-call(bf16[256,512]{1,0:T(8,128)(2,1)S(1)} %pad_maximum_fusion.1.yh, bf16[4,2,512,256]{3,2,1,0:T(8,128)(2,1)S(1)} %get-tuple-element.10.backs), custom_call_target="tpu_custom_call" | custom-call | tf_op jit(solution)/shard_map/output/pallas_call | solution.py:572
  170.1 0.8 copy.21
  (7 shorter events, 0.1 us)
Async XLA Ops:
  0.0 113.5 %copy-start = (bf16[4,256,256]{2,1,0:T(8,128)(2,1)S(1)}, bf16[4,256,256]{2,1,0:T(8,128)(2,1)}, u32[]{:S(2)}) copy-start(bf16[4,256,256]{2,1,0:T(8,128)(2,1)} %param.19) | copy-start | bytes 1572868
  0.0 114.7 %collective-permute-start = (f32[2]{0:T(128)}, f32[2]{0:T(128)S(1)}, u32[]{:S(2)}, u32[]{:S(2)}) collective-permute-start(f32[2]{0:T(128)} %param.21), channel_id=1, source_target_pairs={{0,1},{1,0},{2,3},{3,2},{4,5},{5,4},{6,7},{7,6},{8,9},{9,8},{10,11... | collective-permute-start | bytes 32 | tf_op jit(solution)/shard_map/ppermute | solution.py:536
  4.5 1.2 copy-start.2
  5.7 0.9 copy-start.3
  6.7 0.9 copy-start.4
  7.6 0.9 copy-start.5
  8.6 0.9 copy-start.6
  9.5 0.9 copy-start.7
  10.5 0.9 copy-start.8
  11.4 0.7 copy-start.9
  108.9 1.1 copy-start.1
  110.1 3.4 %copy-start.10 = (f32[256,256]{1,0:T(8,128)S(1)}, f32[256,256]{1,0:T(8,128)}, u32[]{:S(2)}) copy-start(f32[256,256]{1,0:T(8,128)} %slice_convert_fusion.1) | copy-start | bytes 786436
  113.5 3.1 %copy-start.11 = (f32[512,128]{1,0:T(8,128)S(1)}, f32[512,128]{1,0:T(8,128)}, u32[]{:S(2)}) copy-start(f32[512,128]{1,0:T(8,128)} %get-tuple-element.20) | copy-start | bytes 786436
  116.6 2.6 %copy-start.12 = (bf16[256,256]{1,0:T(8,128)(2,1)S(1)}, bf16[256,256]{1,0:T(8,128)(2,1)}, u32[]{:S(2)}) copy-start(bf16[256,256]{1,0:T(8,128)(2,1)} %fusion) | copy-start | bytes 393220

commit v2 on v1

--- a/solution.py
+++ b/solution.py
@@ -262,20 +262,46 @@
     partner = (sp, fs, 1 - tp)
     waits = []
 
-    for d in range(1, nfs):
-        to = lax.rem(fs + d, nfs)
-        for m, mat in enumerate(mats):
+    def send_mat(m):
+        for d in (3, 1, 2):
+            to = lax.rem(fs + d, nfs)
             c = remote(
-                mat.at[:, cols(to // 2, group)], wg.at[fs, m], w_send.at[d - 1, m],
-                w_recv.at[fs, m], (sp, to, tp),
+                mats[m].at[:, cols(to // 2, group)], wg.at[m, fs], w_send.at[d - 1, m],
+                w_recv.at[m, fs], (sp, to, tp),
             )
             c.start()
             waits.append(c)
-    own_w = []
-    for m, mat in enumerate(mats):
-        c = pltpu.make_async_copy(mat.at[:, cols(y, group)], wg.at[fs, m], w_local.at[m])
+        c = pltpu.make_async_copy(mats[m].at[:, cols(y, group)], wg.at[m, fs], w_local.at[m])
         c.start()
-        own_w.append(c)
+        return c
+
+    own_w = [send_mat(0)]
+
+    floats = tok[...].astype(jnp.float32)
+    xn[...] = (
+        floats * lax.rsqrt(jnp.mean(floats * floats, axis=-1, keepdims=True) + eps) * gain[...]
+    ).astype(jnp.bfloat16)
+
+    mine = pl.ds(pl.multiple_of(tp * half, half), half)
+
+    def slot_of(from_y, from_sp):
+        return xg.at[from_y, pl.ds(pl.multiple_of(from_sp * span + tp * half, half), half)]
+
+    moves = [(2, 1), (1, 1), (3, 1), (0, 1), (2, 0), (1, 0), (3, 0)]
+    for i, (dz, dy) in enumerate(moves):
+        to_sp, to_y = lax.rem(sp + dz, nsp), lax.rem(y + dy, 2)
+        c = remote(
+            xn.at[mine, cols(to_sp, feats)], slot_of(y, sp), x_send.at[i],
+            x_recv.at[y, sp], (to_sp, 2 * to_y + x, tp),
+        )
+        c.start()
+        waits.append(c)
+    own_x = pltpu.make_async_copy(
+        xn.at[:, cols(sp, feats)], xg.at[y, pl.ds(pl.multiple_of(sp * span, span), span)], x_local
+    )
+    own_x.start()
+    for m in range(1, 4):
+        own_w.append(send_mat(m))
     for j in range(2):
         for h in range(2):
             to_sp, to_fs = 2 * y + tp, 2 * j + x
@@ -291,89 +317,75 @@
             def _():
                 remote(state.at[j], dst, s_send.at[2 * j + h], s_recv.at[sp], (to_sp, to_fs, h)).start()
 
-    floats = tok[...].astype(jnp.float32)
-    xn[...] = (
-        floats * lax.rsqrt(jnp.mean(floats * floats, axis=-1, keepdims=True) + eps) * gain[...]
-    ).astype(jnp.bfloat16)
-
-    mine = pl.ds(pl.multiple_of(tp * half, half), half)
-    moves = [(dz, dy) for dz in range(nsp) for dy in range(2) if dz or dy]
-    for i, (dz, dy) in enumerate(moves):
-        to_sp, to_y = lax.rem(sp + dz, nsp), lax.rem(y + dy, 2)
-        c = remote(
-            xn.at[mine, cols(to_sp, feats)], xg.at[y, sp, mine], x_send.at[i],
-            x_recv.at[y, sp], (to_sp, 2 * to_y + x, tp),
-        )
-        c.start()
-        waits.append(c)
-    own_x = pltpu.make_async_copy(xn.at[:, cols(sp, feats)], xg.at[y, sp], x_local)
-    own_x.start()
-
-    forwards = []
-    for i, (dz, dy) in enumerate(moves):
-        fr_sp, fr_y = lax.rem(sp + nsp - dz, nsp), lax.rem(y + dy, 2)
-        slot = xg.at[fr_y, fr_sp, mine]
-        remote(slot, slot, x_send.at[i], x_recv.at[fr_y, fr_sp], partner).wait_recv()
-        c = remote(slot, slot, f_send.at[i], f_recv.at[i], partner)
-        c.start()
-        forwards.append(c)
-
     own_b = []
     for b, back in enumerate((pb, rb)):
         c = pltpu.make_async_copy(back, backs.at[fs, b], b_local.at[b])
         c.start()
         own_b.append(c)
-        for d in range(1, nfs):
+        for d in (3, 1, 2):
             to = lax.rem(fs + d, nfs)
             c = remote(back, backs.at[fs, b], b_send.at[d - 1, b], b_recv.at[fs, b], (sp, to, tp))
             c.start()
             waits.append(c)
 
+    forwards = []
+    for i in (3, 5, 6, 4, 1, 2, 0):
+        dz, dy = moves[i]
+        fr_sp, fr_y = lax.rem(sp + nsp - dz, nsp), lax.rem(y + dy, 2)
+        slot = slot_of(fr_y, fr_sp)
+        remote(slot, slot, x_send.at[i], x_recv.at[fr_y, fr_sp], partner).wait_recv()
+        c = remote(slot, slot, f_send.at[i], f_recv.at[i], partner)
+        c.start()
+        forwards.append(c)
     own_x.wait()
-    for c in own_w:
-        c.wait()
     for c in forwards:
         c.wait()
-    for d in range(1, nfs):
-        fr = lax.rem(fs + nfs - d, nfs)
-        for m, mat in enumerate(mats):
+
+    tall = 2 * span
+    for m in range(4):
+        own_w[m].wait()
+        for d in range(1, nfs):
+            fr = lax.rem(fs + nfs - d, nfs)
             remote(
-                mat.at[:, cols(y, group)], wg.at[fr, m], w_send.at[d - 1, m], w_recv.at[fr, m], partner
+                mats[m].at[:, cols(y, group)], wg.at[m, fr], w_send.at[d - 1, m], w_recv.at[m, fr], partner
             ).wait_recv()
-
-    tall = 2 * span
-    for s in range(2):
-        for h in range(2):
-            for m in range(4):
-                acc = jnp.zeros((tall, group), jnp.float32)
-                for f in range(nfs):
-                    lhs = jnp.concatenate(
-                        [xg[s, 2 * h + k, :, f * rows : (f + 1) * rows] for k in range(2)], axis=0
-                    )
-                    acc += jnp.dot(lhs, wg[f, m], preferred_element_type=jnp.float32)
-                part[s, h, :, m * group : (m + 1) * group] = acc.astype(jnp.bfloat16)
-            same = (2 * s + tp == sp) & (tp == h)
-
-            @pl.when(same)
-            def _():
-                pltpu.make_async_copy(part.at[s, h], got.at[sp], p_recv.at[sp]).start()
-
-            @pl.when(jnp.logical_not(same))
-            def _():
-                remote(
-                    part.at[s, h], got.at[sp], p_send.at[2 * s + h], p_recv.at[sp], (2 * s + tp, fs, h)
-                ).start()
-
-    for k in range(nsp):
-        remote(part.at[0, 0], got.at[k], p_send.at[0], p_recv.at[k], partner).wait_recv()
-    total = got[0].astype(jnp.float32)
-    for k in range(1, nsp):
-        total += got[k].astype(jnp.float32)
-    joined[tp] = total.astype(jnp.bfloat16)
-    last = remote(joined.at[tp], joined.at[tp], j_send, j_recv, partner)
-    last.start()
-    last.wait_send()
-    remote(joined.at[1 - tp], joined.at[1 - tp], j_send, j_recv, partner).wait_recv()
+        for s in range(2):
+            acc = jnp.zeros((2 * tall, group), jnp.float32)
+            for f in range(nfs):
+                acc += jnp.dot(
+                    xg[s, :, f * rows : (f + 1) * rows], wg[m, f], preferred_element_type=jnp.float32
+                )
+            part[m, s] = acc.astype(jnp.bfloat16)
+            for h in range(2):
+                same = (2 * s + tp == sp) & (tp == h)
+                src = part.at[m, s, h * tall : (h + 1) * tall]
+
+                @pl.when(same)
+                def _():
+                    pltpu.make_async_copy(src, got.at[m, sp], p_recv.at[m, sp]).start()
+
+                @pl.when(jnp.logical_not(same))
+                def _():
+                    remote(
+                        src, got.at[m, sp], p_send.at[m, 2 * s + h], p_recv.at[m, sp], (2 * s + tp, fs, h)
+                    ).start()
+
+    here = pl.ds(pl.multiple_of(tp * tall, tall), tall)
+    there = pl.ds(pl.multiple_of((1 - tp) * tall, tall), tall)
+    lasts = []
+    for m in range(4):
+        for k in range(nsp):
+            remote(got.at[m, k], got.at[m, k], p_send.at[0, 0], p_recv.at[m, k], partner).wait_recv()
+        total = got[m, 0].astype(jnp.float32)
+        for k in range(1, nsp):
+            total += got[m, k].astype(jnp.float32)
+        joined[m, here] = total.astype(jnp.bfloat16)
+        c = remote(joined.at[m, here], joined.at[m, here], j_send.at[m], j_recv.at[m], partner)
+        c.start()
+        lasts.append(c)
+    for m in range(4):
+        lasts[m].wait_send()
+        remote(joined.at[m, there], joined.at[m, there], j_send.at[m], j_recv.at[m], partner).wait_recv()
 
     for j in range(2):
         for h in range(2):
@@ -388,7 +400,8 @@
 
             @pl.when(jnp.logical_not(same_p))
             def _():
-                remote(part.at[j, h], got.at[0], p_send.at[2 * j + h], p_recv.at[0], partner).wait_send()
+                for m in range(4):
+                    remote(got.at[m, 0], got.at[m, 0], p_send.at[m, 2 * j + h], p_recv.at[m, 0], partner).wait_send()
 
     for k in range(nsp):
         rs = state.shape[1]
@@ -507,7 +520,7 @@
     joined, start, backs = pl.pallas_call(
         project_kernel,
         out_shape=(
-            jax.ShapeDtypeStruct((2, half, 4 * group), bf),
+            jax.ShapeDtypeStruct((4, length, group), bf),
             jax.ShapeDtypeStruct((nsp * rs, group), bf),
             jax.ShapeDtypeStruct((4, 2) + pool_back.shape, bf),
         ),
@@ -515,22 +528,21 @@
         out_specs=(vm, vm, vm),
         scratch_shapes=[
             pltpu.VMEM((span, width), bf),
-            pltpu.VMEM((2, nsp, span, width // nsp), bf),
+            pltpu.VMEM((2, nsp * span, width // nsp), bf),
             pltpu.VMEM((4, 4, rows, group), bf),
-            pltpu.VMEM((2, 2, half, 4 * group), bf),
-            pltpu.VMEM((nsp, half, 4 * group), bf),
+            pltpu.VMEM((4, 2, length, group), bf),
+            pltpu.VMEM((4, nsp, half, group), bf),
             dma((3, 4)), dma((4, 4)), dma((4,)), dma((7,)), dma((2, nsp)), dma,
             dma((7,)), dma((7,)), dma((4,)), dma((nsp,)), dma((3, 2)), dma((4, 2)), dma((2,)),
-            dma((4,)), dma((nsp,)), dma, dma,
+            dma((4, 4)), dma((4, nsp)), dma((4,)), dma((4,)),
         ],
-        compiler_params=pltpu.CompilerParams(has_side_effects=True, vmem_limit_bytes=48 * 2**20),
+        compiler_params=pltpu.CompilerParams(has_side_effects=True, vmem_limit_bytes=60 * 2**20),
         name="project",
     )(
         tok, norm_gain[None, :], pool_proj, query_proj, key_proj, value_proj,
         start_state[0].astype(bf), pool_back, retention_back,
     )
-    whole = joined.reshape(length, 4 * group)
-    mine = joined[tp] if False else lax.dynamic_index_in_dim(joined, tp, 0, keepdims=False)
+    mine = lax.dynamic_slice_in_dim(joined[1], tp * half, half, 0)
     head = 2 * (sp % 2) + y
     local = lax.dynamic_index_in_dim(decay_rate, y, 0, keepdims=False)
     other = lax.ppermute(decay_rate, "tp", [(0, 1), (1, 0)])
@@ -538,7 +550,7 @@
     every = jnp.arange(length, dtype=jnp.int32)
     position = tp * half + jnp.arange(half, dtype=jnp.int32)
 
-    pool_all = jnp.concatenate([jnp.zeros((HALO, group), f32), whole[:, :group].astype(f32)], axis=0)
+    pool_all = jnp.concatenate([jnp.zeros((HALO, group), f32), joined[0].astype(f32)], axis=0)
     extended = lax.dynamic_slice_in_dim(pool_all, tp * half, half + HALO, 0)
     sums = trailing_sums(extended, half)
     windows = jnp.array(window_list, dtype=jnp.int32)
@@ -554,9 +566,9 @@
     cosine, sine = angles_of(every, group // 2)
     my_cos = lax.dynamic_slice_in_dim(cosine, tp * half, half, 0)
     my_sin = lax.dynamic_slice_in_dim(sine, tp * half, half, 0)
-    rq = turned(mine[:, group : 2 * group].astype(f32), my_cos, my_sin)
-    rk = turned(whole[:, 2 * group : 3 * group].astype(f32), cosine, sine) * group ** (-0.5)
-    value = whole[:, 3 * group :].astype(f32)
+    rq = turned(mine.astype(f32), my_cos, my_sin)
+    rk = turned(joined[2].astype(f32), cosine, sine) * group ** (-0.5)
+    value = joined[3].astype(f32)
     gap = (position[:, None] - every[None, :]).astype(f32)
     mask = jnp.where(gap >= 0, jnp.exp(-jnp.maximum(gap, 0.0) * rate), 0.0)
     high = lax.Precision.HIGHEST
@@ -582,7 +594,7 @@
             pltpu.VMEM((nsp, few, 4 * pool_back.shape[1]), bf),
             dma((nsp,)), dma((2, 2)), dma((nsp,)), dma((nsp,)), dma((nsp,)), dma((nsp,)), dma,
         ],
-        compiler_params=pltpu.CompilerParams(has_side_effects=True, vmem_limit_bytes=48 * 2**20),
+        compiler_params=pltpu.CompilerParams(has_side_effects=True, vmem_limit_bytes=60 * 2**20),
         name="output",
     )(yh, backs)[None]
 

time: 173 us -> 163 us (0.942)
  local copies, waits for them, and re-layouts: 12.6 us -> 5.81 us
  Pallas kernels: 148 us -> 145 us
    unnamed x27 -> x5, local copies, waits for them, and re-layouts: 8.65 us -> 1.88 us
  transfers between devices with their start and end apart: 1 -> 1, of which waited for: 0 -> 0; matrix products, arithmetic and copies ran while one was open for 6% -> 5% of each run, Pallas kernels for 57% -> 59%
where the time goes in v2:
time: 163 us; the launch traced here: 161 us
  Pallas kernels  145 us (89%)
  local copies, waits for them, and re-layouts  5.81 us (4%)
  other arithmetic  5.58 us (3%)
  matrix products  3.01 us (2%)
    pallas_call x1, Pallas kernels, paired(): pl.pallas_call(project_kernel, out_shape=(jax.ShapeDtypeStruct((4, length...  95.5 us
    pallas_call x1, Pallas kernels, paired(): pl.pallas_call(output_kernel, out_shape=jax.ShapeDtypeStruct((few, width)...  49.4 us
  transfers between devices with their start and end apart: 1, of which 0 were waited for; matrix products, arithmetic and copies ran while one was open for 5% of the time, Pallas kernels for 59%

profile of v2, /device:TPU:30, one launch (start us, length us, event | category | flops | bytes accessed | tf_op | source)
XLA Modules:
  0.0 160.8 jit_solution(10371550584799728581)
XLA Ops:
  0.0 0.0 copy-start
  0.0 0.0 collective-permute-start
  0.1 1.3 dynamic_slice.36
  1.4 1.2 dynamic_slice.30
  2.7 0.7 minimum_convert_fusion
  3.3 1.5 convert_bitcast_fusion.state
  4.9 95.5 %project.1 = (bf16[4,512,256]{2,1,0:T(8,128)(2,1)}, bf16[256,256]{1,0:T(8,128)(2,1)}, bf16[4,2,512,256]{3,2,1,0:T(8,128)(2,1)}) custom-call(bf16[128,4096]{1,0:T(8,128)(2,1)} %bitcast.25, f32[1,4096]{1,0:T(1,128)} %bitcast.26, bf16[256,512]{1,0:T(8,128)(2,1)} %wp.1, bf16[256,512]{1,0:T(8,128)(2,1)} %wq.1, bf16[256,512]{1,0:T(8,128)(2,1)} %wk.1, ...), custom_call_target="tpu_custom_call" | custom-call | tf_op jit(solution)/shard_map/project/pallas_call | solution.py:520
  100.4 1.2 slice_bitcast_fusion
  101.6 0.8 dynamic_slice.32
  102.4 0.1 fusion.18
  102.5 1.2 multiply_cosine_fusion
  103.7 0.0 copy-done
  103.8 0.5 fusion
  104.3 0.0 copy-start.1
  104.3 0.0 collective-permute-done
  104.3 0.6 dynamic_slice.37
  106.2 0.7 convolution_multiply_fusion
  106.9 1.3 fusion.6
  108.3 0.0 copy-done.1
  108.3 0.4 multiply_reduce_fusion
  108.7 0.1 multiply_convert_fusion
  108.8 0.7 pad_maximum_fusion.1.yh
  109.5 49.4 %output.1 = bf16[64,4096]{1,0:T(8,128)(2,1)} custom-call(bf16[256,512]{1,0:T(8,128)(2,1)} %pad_maximum_fusion.1.yh, bf16[4,2,512,256]{3,2,1,0:T(8,128)(2,1)} %get-tuple-element.10.backs), custom_call_target="tpu_custom_call" | custom-call | tf_op jit(solution)/shard_map/output/pallas_call | solution.py:584
  158.9 1.9 %copy.21 = bf16[1,64,4096]{2,1,0:T(8,128)(2,1)} copy(bf16[1,64,4096]{2,1,0:T(8,128)(2,1)} %bitcast.24) | data formatting | bytes 1048576
  (7 shorter events, 0.1 us)
Async XLA Ops:
  0.0 103.7 %copy-start = (bf16[4,256,256]{2,1,0:T(8,128)(2,1)S(1)}, bf16[4,256,256]{2,1,0:T(8,128)(2,1)}, u32[]{:S(2)}) copy-start(bf16[4,256,256]{2,1,0:T(8,128)(2,1)} %param.19) | copy-start | bytes 1572868
  0.0 104.3 %collective-permute-start = (f32[2]{0:T(128)}, f32[2]{0:T(128)S(1)}, u32[]{:S(2)}, u32[]{:S(2)}) collective-permute-start(f32[2]{0:T(128)} %param.21), channel_id=1, source_target_pairs={{0,1},{1,0},{2,3},{3,2},{4,5},{5,4},{6,7},{7,6},{8,9},{9,8},{10,11... | collective-permute-start | bytes 32 | tf_op jit(solution)/shard_map/ppermute | solution.py:548
  104.3 4.0 %copy-start.1 = (bf16[256,256]{1,0:T(8,128)(2,1)S(1)}, bf16[256,256]{1,0:T(8,128)(2,1)}, u32[]{:S(2)}) copy-start(bf16[256,256]{1,0:T(8,128)(2,1)} %get-tuple-element.9) | copy-start | bytes 393220

commit v3 on v2

--- a/solution.py
+++ b/solution.py
@@ -241,6 +241,13 @@
     )
 
 
+def greet(others):
+    barrier = pltpu.get_barrier_semaphore()
+    for other in others:
+        pl.semaphore_signal(barrier, inc=1, device_id=other, device_id_type=MESH)
+    pl.semaphore_wait(barrier, len(others))
+
+
 def cols(index, size):
     return pl.ds(pl.multiple_of(index * size, size), size)
 
@@ -261,6 +268,13 @@
     mats = (wp, wq, wk, wv)
     partner = (sp, fs, 1 - tp)
     waits = []
+    greet(
+        [
+            (lax.rem(sp + dz, nsp), 2 * lax.rem(y + dy, 2) + x, lax.rem(tp + dt, 2))
+            for dz in range(nsp) for dy in range(2) for dt in range(2) if dz or dy or dt
+        ]
+        + [(sp, 2 * lax.rem(y + dy, 2) + 1 - x, tp) for dy in range(2)]
+    )
 
     def send_mat(m):
         for d in (3, 1, 2):
@@ -287,12 +301,12 @@
     def slot_of(from_y, from_sp):
         return xg.at[from_y, pl.ds(pl.multiple_of(from_sp * span + tp * half, half), half)]
 
-    moves = [(2, 1), (1, 1), (3, 1), (0, 1), (2, 0), (1, 0), (3, 0)]
-    for i, (dz, dy) in enumerate(moves):
-        to_sp, to_y = lax.rem(sp + dz, nsp), lax.rem(y + dy, 2)
+    peer = (sp, 2 * (1 - y) + x, tp)
+    for dz in (2, 1, 3, 0):
+        to_sp = lax.rem(sp + dz, nsp)
         c = remote(
-            xn.at[mine, cols(to_sp, feats)], slot_of(y, sp), x_send.at[i],
-            x_recv.at[y, sp], (to_sp, 2 * to_y + x, tp),
+            xn.at[mine, cols(to_sp, feats)], slot_of(y, sp), x_send.at[dz], x_recv.at[y, sp],
+            (to_sp, fs, tp) if dz else peer,
         )
         c.start()
         waits.append(c)
@@ -329,14 +343,23 @@
             waits.append(c)
 
     forwards = []
-    for i in (3, 5, 6, 4, 1, 2, 0):
-        dz, dy = moves[i]
-        fr_sp, fr_y = lax.rem(sp + nsp - dz, nsp), lax.rem(y + dy, 2)
-        slot = slot_of(fr_y, fr_sp)
-        remote(slot, slot, x_send.at[i], x_recv.at[fr_y, fr_sp], partner).wait_recv()
-        c = remote(slot, slot, f_send.at[i], f_recv.at[i], partner)
+
+    def arrived(from_y, from_sp, order):
+        slot = slot_of(from_y, from_sp)
+        remote(slot, slot, x_send.at[0], x_recv.at[from_y, from_sp], partner).wait_recv()
+        c = remote(slot, slot, f_send.at[order], f_recv.at[order], partner)
         c.start()
         forwards.append(c)
+        return slot
+
+    for dz in (1, 3, 2):
+        fr_sp = lax.rem(sp + nsp - dz, nsp)
+        slot = arrived(y, fr_sp, dz - 1)
+        c = remote(slot, slot, x_send.at[nsp + dz - 1], x_recv.at[y, fr_sp], peer)
+        c.start()
+        waits.append(c)
+    for dz in (0, 1, 3, 2):
+        arrived(1 - y, lax.rem(sp + nsp - dz, nsp), 3 + dz)
     own_x.wait()
     for c in forwards:
         c.wait()
@@ -418,8 +441,8 @@
 
 def output_kernel(
     yh, backs, out,
-    yg, accs, give, take, done,
-    y_send, y_recv, g_send, g_recv, o_send, o_recv, o_local,
+    yg, stage, accs, give, take, done,
+    y_send, y_recv, t_send, t_recv, g_send, g_recv, o_send, o_recv,
 ):
     sp, fs, tp, y, x = where_am_i()
     nsp, nfs = 4, 4
@@ -430,17 +453,39 @@
     across = nfs * block
     partner = (sp, fs, 1 - tp)
     s, p = sp // 2, sp % 2
-    for k in range(nsp):
-        same = (sp == k) & (s == y) & (p == tp)
-
-        @pl.when(same)
-        def _():
-            pltpu.make_async_copy(yh, yg.at[y, tp], y_recv.at[y, tp]).start()
-
-        @pl.when(jnp.logical_not(same))
-        def _():
-            remote(yh, yg.at[y, tp], y_send.at[k], y_recv.at[y, tp], (k, 2 * s + x, p)).start()
-
+    peer = (sp, 2 * (1 - y) + x, tp)
+    greet(
+        [
+            (lax.rem(sp + dz, nsp), fs, lax.rem(tp + dt, 2))
+            for dz in range(nsp) for dt in range(2) if dz or dt
+        ]
+        + [peer]
+    )
+    for dz in (2, 1, 3, 0):
+        k = lax.rem(sp + dz, nsp)
+        for staged, dst, sem in ((False, yg.at[y, tp], y_recv.at[y, tp]), (True, stage.at[tp], t_recv.at[tp])):
+            kind = (s != y) if staged else (s == y)
+            if dz:
+
+                @pl.when(kind)
+                def _():
+                    remote(yh, dst, y_send.at[dz], sem, (k, fs, p)).start()
+            else:
+
+                @pl.when(kind & (p == tp))
+                def _():
+                    pltpu.make_async_copy(yh, dst, sem).start()
+
+                @pl.when(kind & (p != tp))
+                def _():
+                    remote(yh, dst, y_send.at[dz], sem, partner).start()
+
+    passed = []
+    for h in range(2):
+        remote(yh, stage.at[h], y_send.at[0], t_recv.at[h], partner).wait_recv()
+        c = remote(stage.at[h], yg.at[y, h], t_send.at[h], y_recv.at[y, h], peer)
+        c.start()
+        passed.append(c)
     gives = []
     for h in range(2):
         for q in range(2):
@@ -482,11 +527,15 @@
         def _():
             remote(done.at[k], out.at[:, k * across : (k + 1) * across], o_send.at[k], o_recv.at[k], partner).wait_send()
 
-        same = (sp == k) & (s == y) & (p == tp)
-
-        @pl.when(jnp.logical_not(same))
-        def _():
-            remote(yh, yg.at[0, 0], y_send.at[k], y_recv.at[0, 0], partner).wait_send()
+    for dz in range(1, nsp):
+        remote(yh, yg.at[0, 0], y_send.at[dz], y_recv.at[0, 0], partner).wait_send()
+
+    @pl.when(p != tp)
+    def _():
+        remote(yh, yg.at[0, 0], y_send.at[0], y_recv.at[0, 0], partner).wait_send()
+
+    for c in passed:
+        c.wait_send()
 
 
 def turned(values, cosine, sine):
@@ -536,7 +585,7 @@
             dma((7,)), dma((7,)), dma((4,)), dma((nsp,)), dma((3, 2)), dma((4, 2)), dma((2,)),
             dma((4, 4)), dma((4, nsp)), dma((4,)), dma((4,)),
         ],
-        compiler_params=pltpu.CompilerParams(has_side_effects=True, vmem_limit_bytes=60 * 2**20),
+        compiler_params=pltpu.CompilerParams(collective_id=0, has_side_effects=True, vmem_limit_bytes=60 * 2**20),
         name="project",
     )(
         tok, norm_gain[None, :], pool_proj, query_proj, key_proj, value_proj,
@@ -588,13 +637,14 @@
         out_specs=vm,
         scratch_shapes=[
             pltpu.VMEM((2, 2, half, 2 * group), bf),
+            pltpu.VMEM((2, half, 2 * group), bf),
             pltpu.VMEM((length, 4 * pool_back.shape[1]), f32),
             pltpu.VMEM((nsp, few, 4 * pool_back.shape[1]), bf),
             pltpu.VMEM((nsp, few, 4 * pool_back.shape[1]), bf),
             pltpu.VMEM((nsp, few, 4 * pool_back.shape[1]), bf),
-            dma((nsp,)), dma((2, 2)), dma((nsp,)), dma((nsp,)), dma((nsp,)), dma((nsp,)), dma,
+            dma((nsp,)), dma((2, 2)), dma((2,)), dma((2,)), dma((nsp,)), dma((nsp,)), dma((nsp,)), dma((nsp,)),
         ],
-        compiler_params=pltpu.CompilerParams(has_side_effects=True, vmem_limit_bytes=60 * 2**20),
+        compiler_params=pltpu.CompilerParams(collective_id=1, has_side_effects=True, vmem_limit_bytes=60 * 2**20),
         name="output",
     )(yh, backs)[None]
 

time: 163 us -> 183 us (1.12)
  Pallas kernels: 145 us -> 166 us
    pallas_call x1, Pallas kernels: 95.5 us -> 117 us  [paired(): pl.pallas_call(project_kernel, out_shape=(jax.ShapeDtypeStruct((4, length...]
  transfers between devices with their start and end apart: 1 -> 1, of which waited for: 0 -> 0; matrix products, arithmetic and copies ran while one was open for 5% -> 5% of each run, Pallas kernels for 59% -> 64%
where the time goes in v3:
time: 183 us; the launch traced here: 182 us
  Pallas kernels  166 us (91%)
  local copies, waits for them, and re-layouts  5.81 us (3%)
  other arithmetic  5.58 us (3%)
  matrix products  3 us (2%)
    pallas_call x1, Pallas kernels, paired(): pl.pallas_call(project_kernel, out_shape=(jax.ShapeDtypeStruct((4, length...  117 us
    pallas_call x1, Pallas kernels, paired(): pl.pallas_call(output_kernel, out_shape=jax.ShapeDtypeStruct((few, width)...  48.6 us
  transfers between devices with their start and end apart: 1, of which 0 were waited for; matrix products, arithmetic and copies ran while one was open for 5% of the time, Pallas kernels for 64%

profile of v3, /device:TPU:30, one launch (start us, length us, event | category | flops | bytes accessed | tf_op | source)
XLA Modules:
  0.0 181.7 jit_solution(2032933616087641918)
XLA Ops:
  0.0 0.0 copy-start
  0.0 0.0 collective-permute-start
  0.1 1.3 dynamic_slice.36
  1.4 1.2 dynamic_slice.30
  2.7 0.7 minimum_convert_fusion
  3.3 1.5 convert_bitcast_fusion.state
  4.9 117.2 %project.1 = (bf16[4,512,256]{2,1,0:T(8,128)(2,1)}, bf16[256,256]{1,0:T(8,128)(2,1)}, bf16[4,2,512,256]{3,2,1,0:T(8,128)(2,1)}) custom-call(bf16[128,4096]{1,0:T(8,128)(2,1)} %bitcast.25, f32[1,4096]{1,0:T(1,128)} %bitcast.26, bf16[256,512]{1,0:T(8,128)(2,1)} %wp.1, bf16[256,512]{1,0:T(8,128)(2,1)} %wq.1, bf16[256,512]{1,0:T(8,128)(2,1)} %wk.1, ...), custom_call_target="tpu_custom_call" | custom-call | tf_op jit(solution)/shard_map/project/pallas_call | solution.py:569
  122.1 1.2 slice_bitcast_fusion
  123.3 0.8 dynamic_slice.32
  124.0 0.1 fusion.18
  124.2 1.2 multiply_cosine_fusion
  125.4 0.0 copy-done
  125.4 0.5 fusion
  125.9 0.0 copy-start.1
  125.9 0.0 collective-permute-done
  125.9 0.6 dynamic_slice.37
  127.8 0.7 convolution_multiply_fusion
  128.6 1.3 fusion.6
  129.9 0.0 copy-done.1
  129.9 0.4 multiply_reduce_fusion
  130.3 0.1 multiply_convert_fusion
  130.5 0.7 pad_maximum_fusion.1.yh
  131.2 48.6 %output.1 = bf16[64,4096]{1,0:T(8,128)(2,1)} custom-call(bf16[256,512]{1,0:T(8,128)(2,1)} %pad_maximum_fusion.1.yh, bf16[4,2,512,256]{3,2,1,0:T(8,128)(2,1)} %get-tuple-element.10.backs), custom_call_target="tpu_custom_call" | custom-call | tf_op jit(solution)/shard_map/output/pallas_call | solution.py:633
  179.8 1.9 %copy.21 = bf16[1,64,4096]{2,1,0:T(8,128)(2,1)} copy(bf16[1,64,4096]{2,1,0:T(8,128)(2,1)} %bitcast.24) | data formatting | bytes 1048576
  (7 shorter events, 0.1 us)
Async XLA Ops:
  0.0 125.4 %copy-start = (bf16[4,256,256]{2,1,0:T(8,128)(2,1)S(1)}, bf16[4,256,256]{2,1,0:T(8,128)(2,1)}, u32[]{:S(2)}) copy-start(bf16[4,256,256]{2,1,0:T(8,128)(2,1)} %param.19) | copy-start | bytes 1572868
  0.0 125.9 %collective-permute-start = (f32[2]{0:T(128)}, f32[2]{0:T(128)S(1)}, u32[]{:S(2)}, u32[]{:S(2)}) collective-permute-start(f32[2]{0:T(128)} %param.21), channel_id=1, source_target_pairs={{0,1},{1,0},{2,3},{3,2},{4,5},{5,4},{6,7},{7,6},{8,9},{9,8},{10,11... | collective-permute-start | bytes 32 | tf_op jit(solution)/shard_map/ppermute | solution.py:597
  125.9 4.0 %copy-start.1 = (bf16[256,256]{1,0:T(8,128)(2,1)S(1)}, bf16[256,256]{1,0:T(8,128)(2,1)}, u32[]{:S(2)}) copy-start(bf16[256,256]{1,0:T(8,128)(2,1)} %get-tuple-element.9) | copy-start | bytes 393220

commit v4 on v3

--- a/solution.py
+++ b/solution.py
@@ -314,7 +314,24 @@
         xn.at[:, cols(sp, feats)], xg.at[y, pl.ds(pl.multiple_of(sp * span, span), span)], x_local
     )
     own_x.start()
-    for m in range(1, 4):
+    own_w.append(send_mat(1))
+    forwards = []
+
+    def arrived(from_y, from_sp, order):
+        slot = slot_of(from_y, from_sp)
+        remote(slot, slot, x_send.at[0], x_recv.at[from_y, from_sp], partner).wait_recv()
+        c = remote(slot, slot, f_send.at[order], f_recv.at[order], partner)
+        c.start()
+        forwards.append(c)
+        return slot
+
+    for dz in (1, 3, 2):
+        fr_sp = lax.rem(sp + nsp - dz, nsp)
+        slot = arrived(y, fr_sp, dz - 1)
+        c = remote(slot, slot, x_send.at[nsp + dz - 1], x_recv.at[y, fr_sp], peer)
+        c.start()
+        waits.append(c)
+    for m in range(2, 4):
         own_w.append(send_mat(m))
     for j in range(2):
         for h in range(2):
@@ -342,22 +359,6 @@
             c.start()
             waits.append(c)
 
-    forwards = []
-
-    def arrived(from_y, from_sp, order):
-        slot = slot_of(from_y, from_sp)
-        remote(slot, slot, x_send.at[0], x_recv.at[from_y, from_sp], partner).wait_recv()
-        c = remote(slot, slot, f_send.at[order], f_recv.at[order], partner)
-        c.start()
-        forwards.append(c)
-        return slot
-
-    for dz in (1, 3, 2):
-        fr_sp = lax.rem(sp + nsp - dz, nsp)
-        slot = arrived(y, fr_sp, dz - 1)
-        c = remote(slot, slot, x_send.at[nsp + dz - 1], x_recv.at[y, fr_sp], peer)
-        c.start()
-        waits.append(c)
     for dz in (0, 1, 3, 2):
         arrived(1 - y, lax.rem(sp + nsp - dz, nsp), 3 + dz)
     own_x.wait()
@@ -461,81 +462,105 @@
         ]
         + [peer]
     )
-    for dz in (2, 1, 3, 0):
-        k = lax.rem(sp + dz, nsp)
-        for staged, dst, sem in ((False, yg.at[y, tp], y_recv.at[y, tp]), (True, stage.at[tp], t_recv.at[tp])):
-            kind = (s != y) if staged else (s == y)
-            if dz:
-
-                @pl.when(kind)
-                def _():
-                    remote(yh, dst, y_send.at[dz], sem, (k, fs, p)).start()
-            else:
-
-                @pl.when(kind & (p == tp))
-                def _():
-                    pltpu.make_async_copy(yh, dst, sem).start()
-
-                @pl.when(kind & (p != tp))
-                def _():
-                    remote(yh, dst, y_send.at[dz], sem, partner).start()
+    few2 = half // 2
+    for c in range(2):
+        part = yh.at[c * few2 : (c + 1) * few2]
+        for dz in (2, 1, 3, 0):
+            k = lax.rem(sp + dz, nsp)
+            for staged, dst, sem in (
+                (False, yg.at[y, tp, c], y_recv.at[y, tp, c]), (True, stage.at[tp, c], t_recv.at[tp, c])
+            ):
+                kind = (s != y) if staged else (s == y)
+                if dz:
+
+                    @pl.when(kind)
+                    def _():
+                        remote(part, dst, y_send.at[dz, c], sem, (k, fs, p)).start()
+                else:
+
+                    @pl.when(kind & (p == tp))
+                    def _():
+                        pltpu.make_async_copy(part, dst, sem).start()
+
+                    @pl.when(kind & (p != tp))
+                    def _():
+                        remote(part, dst, y_send.at[dz, c], sem, partner).start()
 
     passed = []
-    for h in range(2):
-        remote(yh, stage.at[h], y_send.at[0], t_recv.at[h], partner).wait_recv()
-        c = remote(stage.at[h], yg.at[y, h], t_send.at[h], y_recv.at[y, h], peer)
-        c.start()
-        passed.append(c)
-    gives = []
-    for h in range(2):
-        for q in range(2):
-            remote(yh, yg.at[q, h], y_send.at[0], y_recv.at[q, h], partner).wait_recv()
-        for f in range(nfs):
-            acc = jnp.zeros((half, block), jnp.float32)
+
+    def forward(c):
+        for h in range(2):
+            slot = stage.at[h, c]
+            remote(slot, slot, y_send.at[0, 0], t_recv.at[h, c], partner).wait_recv()
+            move = remote(slot, yg.at[y, h, c], t_send.at[h, c], y_recv.at[y, h, c], peer)
+            move.start()
+            passed.append(move)
+
+    def multiply(c):
+        gives = []
+        for h in range(2):
             for q in range(2):
-                for b in range(2):
-                    acc += jnp.dot(
-                        yg[q, h, :, b * group : (b + 1) * group],
-                        backs[f, b, q * group : (q + 1) * group, :],
-                        preferred_element_type=jnp.float32,
-                    )
-            accs[h * half : (h + 1) * half, f * block : (f + 1) * block] = acc
-        for k in (2 * h, 2 * h + 1):
-            off = pl.multiple_of(k * 2 * few + (1 - tp) * few, few)
-            give[k] = accs[pl.ds(off, few), :].astype(jnp.bfloat16)
-            c = remote(give.at[k], take.at[k], g_send.at[k], g_recv.at[k], partner)
-            c.start()
-            gives.append(c)
+                slot = yg.at[q, h, c]
+                remote(slot, slot, y_send.at[0, 0], y_recv.at[q, h, c], partner).wait_recv()
+            k = 2 * h + c
+            for f in range(nfs):
+                acc = jnp.zeros((few2, block), jnp.float32)
+                for q in range(2):
+                    for b in range(2):
+                        acc += jnp.dot(
+                            yg[q, h, c, :, b * group : (b + 1) * group],
+                            backs[f, b, q * group : (q + 1) * group, :],
+                            preferred_element_type=jnp.float32,
+                        )
+                accs[k, :, f * block : (f + 1) * block] = acc
+            give[k] = accs[k, pl.ds(pl.multiple_of((1 - tp) * few, few), few), :].astype(jnp.bfloat16)
+            move = remote(give.at[k], take.at[k], g_send.at[k], g_recv.at[k], partner)
+            move.start()
+            gives.append(move)
+        return gives
+
+    def finish(c, gives):
+        for h in range(2):
+            k = 2 * h + c
+            gives[h].wait()
+            own = accs[k, pl.ds(pl.multiple_of(tp * few, few), few), :]
+            done[k] = (own + take[k].astype(jnp.float32)).astype(jnp.bfloat16)
+            dst = out.at[:, cols(sp, across)]
+
+            @pl.when(sp == k)
+            def _():
+                pltpu.make_async_copy(done.at[k], dst, o_recv.at[sp]).start()
+
+            @pl.when(sp != k)
+            def _():
+                remote(done.at[k], dst, o_send.at[k], o_recv.at[sp], (k, fs, tp)).start()
+
+    forward(0)
+    first = multiply(0)
+    finish(0, first)
+    forward(1)
+    second = multiply(1)
+    finish(1, second)
+
     for k in range(nsp):
-        gives[k].wait()
-        off = pl.multiple_of(k * 2 * few + tp * few, few)
-        done[k] = (accs[pl.ds(off, few), :] + take[k].astype(jnp.float32)).astype(jnp.bfloat16)
-        dst = out.at[:, cols(sp, across)]
-
-        @pl.when(sp == k)
-        def _():
-            pltpu.make_async_copy(done.at[k], dst, o_recv.at[sp]).start()
+        view = out.at[:, k * across : (k + 1) * across]
+        remote(done.at[k], view, o_send.at[k], o_recv.at[k], partner).wait_recv()
 
         @pl.when(sp != k)
         def _():
-            remote(done.at[k], dst, o_send.at[k], o_recv.at[sp], (k, fs, tp)).start()
-
-    for k in range(nsp):
-        remote(done.at[k], out.at[:, k * across : (k + 1) * across], o_send.at[k], o_recv.at[k], partner).wait_recv()
-
-        @pl.when(sp != k)
+            remote(done.at[k], view, o_send.at[k], o_recv.at[k], partner).wait_send()
+
+    for c in range(2):
+        slot = yg.at[0, 0, c]
+        for dz in range(1, nsp):
+            remote(slot, slot, y_send.at[dz, c], y_recv.at[0, 0, c], partner).wait_send()
+
+        @pl.when(p != tp)
         def _():
-            remote(done.at[k], out.at[:, k * across : (k + 1) * across], o_send.at[k], o_recv.at[k], partner).wait_send()
-
-    for dz in range(1, nsp):
-        remote(yh, yg.at[0, 0], y_send.at[dz], y_recv.at[0, 0], partner).wait_send()
-
-    @pl.when(p != tp)
-    def _():
-        remote(yh, yg.at[0, 0], y_send.at[0], y_recv.at[0, 0], partner).wait_send()
-
-    for c in passed:
-        c.wait_send()
+            remote(slot, slot, y_send.at[0, c], y_recv.at[0, 0, c], partner).wait_send()
+
+    for move in passed:
+        move.wait_send()
 
 
 def turned(values, cosine, sine):
@@ -636,13 +661,13 @@
         in_specs=[vm, vm],
         out_specs=vm,
         scratch_shapes=[
-            pltpu.VMEM((2, 2, half, 2 * group), bf),
-            pltpu.VMEM((2, half, 2 * group), bf),
-            pltpu.VMEM((length, 4 * pool_back.shape[1]), f32),
+            pltpu.VMEM((2, 2, 2, span, 2 * group), bf),
+            pltpu.VMEM((2, 2, span, 2 * group), bf),
+            pltpu.VMEM((nsp, span, 4 * pool_back.shape[1]), f32),
             pltpu.VMEM((nsp, few, 4 * pool_back.shape[1]), bf),
             pltpu.VMEM((nsp, few, 4 * pool_back.shape[1]), bf),
             pltpu.VMEM((nsp, few, 4 * pool_back.shape[1]), bf),
-            dma((nsp,)), dma((2, 2)), dma((2,)), dma((2,)), dma((nsp,)), dma((nsp,)), dma((nsp,)), dma((nsp,)),
+            dma((nsp, 2)), dma((2, 2, 2)), dma((2, 2)), dma((2, 2)), dma((nsp,)), dma((nsp,)), dma((nsp,)), dma((nsp,)),
         ],
         compiler_params=pltpu.CompilerParams(collective_id=1, has_side_effects=True, vmem_limit_bytes=60 * 2**20),
         name="output",

time: 183 us -> 163 us (0.89)
  Pallas kernels: 166 us -> 147 us
    pallas_call x1, Pallas kernels: 117 us -> 99.6 us  [paired(): pl.pallas_call(project_kernel, out_shape=(jax.ShapeDtypeStruct((4, length...]
  transfers between devices with their start and end apart: 1 -> 1, of which waited for: 0 -> 0; matrix products, arithmetic and copies ran while one was open for 5% -> 5% of each run, Pallas kernels for 64% -> 61%
where the time goes in v4:
time: 163 us
  Pallas kernels  147 us (90%)
  local copies, waits for them, and re-layouts  5.81 us (4%)
  other arithmetic  5.58 us (3%)
  matrix products  3 us (2%)
    pallas_call x1, Pallas kernels, paired(): pl.pallas_call(project_kernel, out_shape=(jax.ShapeDtypeStruct((4, length...  99.6 us
    pallas_call x1, Pallas kernels, paired(): pl.pallas_call(output_kernel, out_shape=jax.ShapeDtypeStruct((few, width)...  47.1 us
  transfers between devices with their start and end apart: 1, of which 0 were waited for; matrix products, arithmetic and copies ran while one was open for 5% of the time, Pallas kernels for 61%

profile of v4, /device:TPU:30, one launch (start us, length us, event | category | flops | bytes accessed | tf_op | source)
XLA Modules:
  0.0 162.6 jit_solution(5216474160181830068)
XLA Ops:
  0.0 0.0 copy-start
  0.0 0.0 collective-permute-start
  0.1 1.3 dynamic_slice.36
  1.4 1.2 dynamic_slice.30
  2.7 0.7 minimum_convert_fusion
  3.3 1.5 convert_bitcast_fusion.state
  4.9 99.6 %project.1 = (bf16[4,512,256]{2,1,0:T(8,128)(2,1)}, bf16[256,256]{1,0:T(8,128)(2,1)}, bf16[4,2,512,256]{3,2,1,0:T(8,128)(2,1)}) custom-call(bf16[128,4096]{1,0:T(8,128)(2,1)} %bitcast.25, f32[1,4096]{1,0:T(1,128)} %bitcast.26, bf16[256,512]{1,0:T(8,128)(2,1)} %wp.1, bf16[256,512]{1,0:T(8,128)(2,1)} %wq.1, bf16[256,512]{1,0:T(8,128)(2,1)} %wk.1, ...), custom_call_target="tpu_custom_call" | custom-call | tf_op jit(solution)/shard_map/project/pallas_call | solution.py:594
  104.5 1.2 slice_bitcast_fusion
  105.7 0.8 dynamic_slice.32
  106.5 0.1 fusion.18
  106.6 1.2 multiply_cosine_fusion
  107.9 0.0 copy-done
  107.9 0.5 fusion
  108.4 0.0 copy-start.1
  108.4 0.0 collective-permute-done
  108.4 0.6 dynamic_slice.37
  110.3 0.7 convolution_multiply_fusion
  111.0 1.3 fusion.6
  112.4 0.0 copy-done.1
  112.4 0.4 multiply_reduce_fusion
  112.8 0.1 multiply_convert_fusion
  112.9 0.7 pad_maximum_fusion.1.yh
  113.6 47.1 %output.1 = bf16[64,4096]{1,0:T(8,128)(2,1)} custom-call(bf16[256,512]{1,0:T(8,128)(2,1)} %pad_maximum_fusion.1.yh, bf16[4,2,512,256]{3,2,1,0:T(8,128)(2,1)} %get-tuple-element.10.backs), custom_call_target="tpu_custom_call" | custom-call | tf_op jit(solution)/shard_map/output/pallas_call | solution.py:658
  160.7 1.9 %copy.21 = bf16[1,64,4096]{2,1,0:T(8,128)(2,1)} copy(bf16[1,64,4096]{2,1,0:T(8,128)(2,1)} %bitcast.24) | data formatting | bytes 1048576
  (7 shorter events, 0.1 us)
Async XLA Ops:
  0.0 107.9 %copy-start = (bf16[4,256,256]{2,1,0:T(8,128)(2,1)S(1)}, bf16[4,256,256]{2,1,0:T(8,128)(2,1)}, u32[]{:S(2)}) copy-start(bf16[4,256,256]{2,1,0:T(8,128)(2,1)} %param.19) | copy-start | bytes 1572868
  0.0 108.4 %collective-permute-start = (f32[2]{0:T(128)}, f32[2]{0:T(128)S(1)}, u32[]{:S(2)}, u32[]{:S(2)}) collective-permute-start(f32[2]{0:T(128)} %param.21), channel_id=1, source_target_pairs={{0,1},{1,0},{2,3},{3,2},{4,5},{5,4},{6,7},{7,6},{8,9},{9,8},{10,11... | collective-permute-start | bytes 32 | tf_op jit(solution)/shard_map/ppermute | solution.py:622
  108.4 4.0 %copy-start.1 = (bf16[256,256]{1,0:T(8,128)(2,1)S(1)}, bf16[256,256]{1,0:T(8,128)(2,1)}, u32[]{:S(2)}) copy-start(bf16[256,256]{1,0:T(8,128)(2,1)} %get-tuple-element.9) | copy-start | bytes 393220

commit v5 on v4

--- a/solution.py
+++ b/solution.py
@@ -314,7 +314,6 @@
         xn.at[:, cols(sp, feats)], xg.at[y, pl.ds(pl.multiple_of(sp * span, span), span)], x_local
     )
     own_x.start()
-    own_w.append(send_mat(1))
     forwards = []
 
     def arrived(from_y, from_sp, order):
@@ -331,7 +330,7 @@
         c = remote(slot, slot, x_send.at[nsp + dz - 1], x_recv.at[y, fr_sp], peer)
         c.start()
         waits.append(c)
-    for m in range(2, 4):
+    for m in range(1, 4):
         own_w.append(send_mat(m))
     for j in range(2):
         for h in range(2):

time: 163 us -> 151 us (0.926)
  Pallas kernels: 147 us -> 135 us
    pallas_call x1, Pallas kernels: 99.6 us -> 87.8 us  [paired(): pl.pallas_call(project_kernel, out_shape=(jax.ShapeDtypeStruct((4, length...]
  transfers between devices with their start and end apart: 1 -> 1, of which waited for: 0 -> 0; matrix products, arithmetic and copies ran while one was open for 5% -> 6% of each run, Pallas kernels for 61% -> 58%
where the time goes in v5:
time: 151 us
  Pallas kernels  135 us (89%)
  local copies, waits for them, and re-layouts  5.81 us (4%)
  other arithmetic  5.58 us (4%)
  matrix products  3.01 us (2%)
    pallas_call x1, Pallas kernels, paired(): pl.pallas_call(project_kernel, out_shape=(jax.ShapeDtypeStruct((4, length...  87.8 us
    pallas_call x1, Pallas kernels, paired(): pl.pallas_call(output_kernel, out_shape=jax.ShapeDtypeStruct((few, width)...  47.1 us
  transfers between devices with their start and end apart: 1, of which 0 were waited for; matrix products, arithmetic and copies ran while one was open for 6% of the time, Pallas kernels for 58%

profile of v5, /device:TPU:30, one launch (start us, length us, event | category | flops | bytes accessed | tf_op | source)
XLA Modules:
  0.0 150.7 jit_solution(13236923857188897295)
XLA Ops:
  0.0 0.0 copy-start
  0.0 0.0 collective-permute-start
  0.1 1.3 dynamic_slice.36
  1.4 1.2 dynamic_slice.30
  2.7 0.7 minimum_convert_fusion
  3.3 1.5 %convert_bitcast_fusion.state = bf16[2,64,256]{2,1,0:T(8,128)(2,1)} fusion(f32[1,2,64,256]{3,2,1,0:T(8,128)} %param.22), kind=kLoop, calls=%fused_computation.50 | loop fusion | flops 32768 | bytes 196608 | tf_op jit(solution)/shard_map/convert_element_type | solution.py:616
  4.9 87.8 %project.1 = (bf16[4,512,256]{2,1,0:T(8,128)(2,1)}, bf16[256,256]{1,0:T(8,128)(2,1)}, bf16[4,2,512,256]{3,2,1,0:T(8,128)(2,1)}) custom-call(bf16[128,4096]{1,0:T(8,128)(2,1)} %bitcast.25, f32[1,4096]{1,0:T(1,128)} %bitcast.26, bf16[256,512]{1,0:T(8,128)(2,1)} %wp.1, bf16[256,512]{1,0:T(8,128)(2,1)} %wq.1, bf16[256,512]{1,0:T(8,128)(2,1)} %wk.1, ...), custom_call_target="tpu_custom_call" | custom-call | tf_op jit(solution)/shard_map/project/pallas_call | solution.py:593
  92.7 1.2 slice_bitcast_fusion
  93.9 0.8 dynamic_slice.32
  94.6 0.1 fusion.18
  94.8 1.2 multiply_cosine_fusion
  96.0 0.0 copy-done
  96.0 0.5 fusion
  96.5 0.0 copy-start.1
  96.5 0.0 collective-permute-done
  96.5 0.6 dynamic_slice.37
  98.4 0.7 convolution_multiply_fusion
  99.2 1.3 fusion.6
  100.5 0.0 copy-done.1
  100.5 0.4 multiply_reduce_fusion
  100.9 0.1 multiply_convert_fusion
  101.0 0.7 pad_maximum_fusion.1.yh
  101.8 47.1 %output.1 = bf16[64,4096]{1,0:T(8,128)(2,1)} custom-call(bf16[256,512]{1,0:T(8,128)(2,1)} %pad_maximum_fusion.1.yh, bf16[4,2,512,256]{3,2,1,0:T(8,128)(2,1)} %get-tuple-element.10.backs), custom_call_target="tpu_custom_call" | custom-call | tf_op jit(solution)/shard_map/output/pallas_call | solution.py:657
  148.9 1.9 %copy.21 = bf16[1,64,4096]{2,1,0:T(8,128)(2,1)} copy(bf16[1,64,4096]{2,1,0:T(8,128)(2,1)} %bitcast.24) | data formatting | bytes 1048576
  (7 shorter events, 0.1 us)
Async XLA Ops:
  0.0 96.0 %copy-start = (bf16[4,256,256]{2,1,0:T(8,128)(2,1)S(1)}, bf16[4,256,256]{2,1,0:T(8,128)(2,1)}, u32[]{:S(2)}) copy-start(bf16[4,256,256]{2,1,0:T(8,128)(2,1)} %param.19) | copy-start | bytes 1572868
  0.0 96.5 %collective-permute-start = (f32[2]{0:T(128)}, f32[2]{0:T(128)S(1)}, u32[]{:S(2)}, u32[]{:S(2)}) collective-permute-start(f32[2]{0:T(128)} %param.21), channel_id=1, source_target_pairs={{0,1},{1,0},{2,3},{3,2},{4,5},{5,4},{6,7},{7,6},{8,9},{9,8},{10,11... | collective-permute-start | bytes 32 | tf_op jit(solution)/shard_map/ppermute | solution.py:621
  96.5 4.0 %copy-start.1 = (bf16[256,256]{1,0:T(8,128)(2,1)S(1)}, bf16[256,256]{1,0:T(8,128)(2,1)}, u32[]{:S(2)}) copy-start(bf16[256,256]{1,0:T(8,128)(2,1)} %get-tuple-element.9) | copy-start | bytes 393220

commit v6 on v5

--- a/solution.py
+++ b/solution.py
@@ -358,11 +358,10 @@
             c.start()
             waits.append(c)
 
-    for dz in (0, 1, 3, 2):
-        arrived(1 - y, lax.rem(sp + nsp - dz, nsp), 3 + dz)
     own_x.wait()
     for c in forwards:
         c.wait()
+    early = len(forwards)
 
     tall = 2 * span
     for m in range(4):
@@ -372,7 +371,12 @@
             remote(
                 mats[m].at[:, cols(y, group)], wg.at[m, fr], w_send.at[d - 1, m], w_recv.at[m, fr], partner
             ).wait_recv()
-        for s in range(2):
+        for s in (y, 1 - y):
+            if m == 0 and s is not y:
+                for dz in (0, 1, 3, 2):
+                    arrived(1 - y, lax.rem(sp + nsp - dz, nsp), 3 + dz)
+                for c in forwards[early:]:
+                    c.wait()
             acc = jnp.zeros((2 * tall, group), jnp.float32)
             for f in range(nfs):
                 acc += jnp.dot(

time: 151 us -> 146 us (0.967)
  Pallas kernels: 135 us -> 130 us
    pallas_call x1, Pallas kernels: 87.8 us -> 81.7 us  [paired(): pl.pallas_call(project_kernel, out_shape=(jax.ShapeDtypeStruct((4, length...]
  transfers between devices with their start and end apart: 1 -> 1, of which waited for: 0 -> 0; matrix products, arithmetic and copies ran while one was open for 6% -> 6% of each run, Pallas kernels for 58% -> 56%
where the time goes in v6:
time: 146 us
  Pallas kernels  130 us (89%)
  local copies, waits for them, and re-layouts  5.81 us (4%)
  other arithmetic  5.58 us (4%)
  matrix products  3 us (2%)
  between operations  1.46 us (1%)
    pallas_call x1, Pallas kernels, paired(): pl.pallas_call(project_kernel, out_shape=(jax.ShapeDtypeStruct((4, length...  81.7 us
    pallas_call x1, Pallas kernels, paired(): pl.pallas_call(output_kernel, out_shape=jax.ShapeDtypeStruct((few, width)...  48 us
  transfers between devices with their start and end apart: 1, of which 0 were waited for; matrix products, arithmetic and copies ran while one was open for 6% of the time, Pallas kernels for 56%

profile of v6, /device:TPU:30, one launch (start us, length us, event | category | flops | bytes accessed | tf_op | source)
XLA Modules:
  0.0 145.6 jit_solution(14646438877943453576)
XLA Ops:
  0.0 0.0 copy-start
  0.0 0.0 collective-permute-start
  0.1 1.3 dynamic_slice.36
  1.4 1.2 dynamic_slice.30
  2.7 0.7 minimum_convert_fusion
  3.3 1.5 %convert_bitcast_fusion.state = bf16[2,64,256]{2,1,0:T(8,128)(2,1)} fusion(f32[1,2,64,256]{3,2,1,0:T(8,128)} %param.22), kind=kLoop, calls=%fused_computation.50 | loop fusion | flops 32768 | bytes 196608 | tf_op jit(solution)/shard_map/convert_element_type | solution.py:620
  4.9 81.7 %project.1 = (bf16[4,512,256]{2,1,0:T(8,128)(2,1)}, bf16[256,256]{1,0:T(8,128)(2,1)}, bf16[4,2,512,256]{3,2,1,0:T(8,128)(2,1)}) custom-call(bf16[128,4096]{1,0:T(8,128)(2,1)} %bitcast.25, f32[1,4096]{1,0:T(1,128)} %bitcast.26, bf16[256,512]{1,0:T(8,128)(2,1)} %wp.1, bf16[256,512]{1,0:T(8,128)(2,1)} %wq.1, bf16[256,512]{1,0:T(8,128)(2,1)} %wk.1, ...), custom_call_target="tpu_custom_call" | custom-call | tf_op jit(solution)/shard_map/project/pallas_call | solution.py:597
  86.6 1.2 slice_bitcast_fusion
  87.8 0.8 dynamic_slice.32
  88.6 0.1 fusion.18
  88.7 1.2 multiply_cosine_fusion
  89.9 0.0 copy-done
  89.9 0.5 fusion
  90.5 0.0 copy-start.1
  90.5 0.0 collective-permute-done
  90.5 0.6 dynamic_slice.37
  92.3 0.7 convolution_multiply_fusion
  93.1 1.3 fusion.6
  94.4 0.0 copy-done.1
  94.5 0.4 multiply_reduce_fusion
  94.9 0.1 multiply_convert_fusion
  95.0 0.7 pad_maximum_fusion.1.yh
  95.7 48.0 %output.1 = bf16[64,4096]{1,0:T(8,128)(2,1)} custom-call(bf16[256,512]{1,0:T(8,128)(2,1)} %pad_maximum_fusion.1.yh, bf16[4,2,512,256]{3,2,1,0:T(8,128)(2,1)} %get-tuple-element.10.backs), custom_call_target="tpu_custom_call" | custom-call | tf_op jit(solution)/shard_map/output/pallas_call | solution.py:661
  143.7 1.9 %copy.21 = bf16[1,64,4096]{2,1,0:T(8,128)(2,1)} copy(bf16[1,64,4096]{2,1,0:T(8,128)(2,1)} %bitcast.24) | data formatting | bytes 1048576
  (7 shorter events, 0.1 us)
Async XLA Ops:
  0.0 89.9 %copy-start = (bf16[4,256,256]{2,1,0:T(8,128)(2,1)S(1)}, bf16[4,256,256]{2,1,0:T(8,128)(2,1)}, u32[]{:S(2)}) copy-start(bf16[4,256,256]{2,1,0:T(8,128)(2,1)} %param.19) | copy-start | bytes 1572868
  0.0 90.5 %collective-permute-start = (f32[2]{0:T(128)}, f32[2]{0:T(128)S(1)}, u32[]{:S(2)}, u32[]{:S(2)}) collective-permute-start(f32[2]{0:T(128)} %param.21), channel_id=1, source_target_pairs={{0,1},{1,0},{2,3},{3,2},{4,5},{5,4},{6,7},{7,6},{8,9},{9,8},{10,11... | collective-permute-start | bytes 32 | tf_op jit(solution)/shard_map/ppermute | solution.py:625
  90.5 4.0 %copy-start.1 = (bf16[256,256]{1,0:T(8,128)(2,1)S(1)}, bf16[256,256]{1,0:T(8,128)(2,1)}, u32[]{:S(2)}) copy-start(bf16[256,256]{1,0:T(8,128)(2,1)} %get-tuple-element.9) | copy-start | bytes 393220
